TPU v7x, 256 devices: a whole 4x4x8 slice. The times are simulated.
256 devices in a mesh: vp: 16 (over y, x), dp: 16 (over z, core).
Axes of the slice: x: 4, y: 4, z: 8, core: 2. Of those that a mesh axis runs over, the one named last changes fastest.
Arguments:
- hidden_act: bfloat16 [8192, 8192], P('dp', 'vp'), may hold values from 0 to 36
- down_weight: bfloat16 [8192, 2048], P('vp'), may hold values from -0.0625 to 0.0625
- residual: bfloat16 [8192, 2048], P(('dp', 'vp')), may hold values from -300 to 300
- post_gain: float32 [2048], replicated, may hold values from 0.1 to 1.9
- final_gain: float32 [2048], replicated, may hold values from 0.1 to 1.9
- vocab: bfloat16 [2048, 32768], P(None, 'vp'), may hold values from -0.33 to 0.33
- vocab_bias: float32 [32768], P('vp'), may hold values from -2.5 to 2.5
- target_ids: int32 [8192, 4], P('dp'), may hold values from 0 to 32767
- target_weights: float32 [8192, 4], P('dp'), may hold values from 0 to 1, as said below
Outputs:
- losses: float32 [8192], P(('dp', 'vp'))
- stream_grad: float32 [8192, 2048], P(('dp', 'vp'))
- vocab_grad: float32 [2048, 32768], P('dp', 'vp')
Inputs may be any that keep to these rules, and one draw needn't show every extreme that they name: `target_weights`: the 4 weights of a token add up to one.
All inputs are finite; a program needn't handle non-finite values.
Results may differ from a plain program's by a relative error of at most 0.01225.
Values may be sent and summed in bfloat16 or wider, within the bound.
No kernel may reach another device: no remote copies, remote signals or barrier semaphores. Data moves between devices by JAX's collectives and lax.ppermute only.
A program may use at most 128 MiB of HBM per device.

v0:
```python
import jax
import jax.numpy as jnp
from jax import lax
from jax.experimental import pallas as pl
from jax.experimental.pallas import tpu as pltpu
from jax.sharding import Mesh
from jax.sharding import PartitionSpec as P


F32 = jnp.float32
BF16 = jnp.bfloat16
VP = ("y", "x")
DP = ("z", "c")
DP_VP = ("z", "c", "y", "x")

epsilon = 1e-06
z_weight = 0.001
loss_scale = 32.0


def exchange(parts, axis):
    return lax.all_to_all(parts, axis, split_axis=0, concat_axis=0, tiled=True)


def summed_over(rows, axis):
    size = lax.axis_size(axis)
    parts = rows.astype(BF16).reshape(size, rows.shape[0] // size, rows.shape[1])
    return jnp.sum(exchange(parts, axis).astype(F32), axis=0)


def copied_over(rows, axis):
    size = lax.axis_size(axis)
    copies = jnp.broadcast_to(rows, (size, *rows.shape))
    return exchange(copies, axis).reshape(size * rows.shape[0], rows.shape[1])


def inverse_rms(values):
    return lax.rsqrt(jnp.mean(values * values, axis=-1, keepdims=True) + epsilon)


def call(kernel, grid, in_specs, out_specs, out_shape, operands, flops, after=(), scratch=(), scalars=None):
    lead = 0 if scalars is None else 1
    used = len(operands)

    def body(*refs):
        kernel(*refs[: lead + used], *refs[lead + used + len(after) :])

    moved = sum(x.size * x.dtype.itemsize for x in operands)
    return pl.pallas_call(
        body,
        grid_spec=pltpu.PrefetchScalarGridSpec(
            num_scalar_prefetch=lead,
            grid=grid,
            in_specs=list(in_specs) + [pl.BlockSpec(memory_space=pl.ANY)] * len(after),
            out_specs=out_specs,
            scratch_shapes=scratch,
        ),
        out_shape=out_shape,
        cost_estimate=pl.CostEstimate(flops=flops, bytes_accessed=moved, transcendentals=0),
    )(*(() if scalars is None else (scalars,)), *operands, *after)


LANES = 128
SCORE_BLOCK = 512


def wanted_matrix(ids, weights, columns, after):
    tokens = ids.shape[0]
    rows = 128

    def kernel(ids_ref, weights_ref, out_ref):
        wide = (rows, LANES)
        at_ids = [jnp.broadcast_to(ids_ref[:, k : k + 1], wide) for k in range(ids.shape[1])]
        at_weights = [jnp.broadcast_to(weights_ref[:, k : k + 1], wide) for k in range(ids.shape[1])]
        lane = lax.broadcasted_iota(jnp.int32, wide, 1)
        for at in range(0, columns, LANES):
            found = jnp.zeros(wide, F32)
            for k in range(ids.shape[1]):
                found = found + jnp.where(at_ids[k] == lane + at, at_weights[k], 0.0)
            out_ref[:, at : at + LANES] = found

    def block(shape):
        return pl.BlockSpec((rows, shape[1]), lambda i: (i, 0))

    return call(
        kernel,
        (tokens // rows,),
        [block(ids.shape), block(weights.shape)],
        block((tokens, columns)),
        jax.ShapeDtypeStruct((tokens, columns), F32),
        [ids, weights],
        8000 * tokens * columns // 1000,
        after,
    )


def turned(x, after):
    rows = 256

    def kernel(x_ref, out_ref):
        out_ref[...] = x_ref[...].T

    return call(
        kernel,
        (x.shape[0] // rows,),
        [pl.BlockSpec((rows, x.shape[1]), lambda i: (i, 0))],
        pl.BlockSpec((x.shape[1], rows), lambda i: (0, i)),
        jax.ShapeDtypeStruct(x.shape[::-1], x.dtype),
        [x],
        2000 * x.size,
        after,
    )


HBM = pl.BlockSpec(memory_space=pl.ANY)


def scored(rows, vocab, bias, wanted):
    tokens, width = rows.shape
    columns = vocab.shape[1]
    blocks = columns // SCORE_BLOCK

    def kernel(rows_hbm, vocab_hbm, bias_ref, wanted_hbm, scores_hbm, stats_ref, rows_in, vocab_in, wanted_in, out, sems):
        def across(j):
            return pl.ds(j * SCORE_BLOCK, SCORE_BLOCK)

        load_rows = pltpu.make_async_copy(rows_hbm, rows_in, sems.at[3, 0])
        load_vocab = [
            pltpu.make_async_copy(vocab_hbm.at[:, across(j)], vocab_in.at[j], sems.at[0, j])
            for j in range(blocks)
        ]
        load_wanted = [
            pltpu.make_async_copy(wanted_hbm.at[:, across(j)], wanted_in.at[j], sems.at[1, j])
            for j in range(blocks)
        ]
        store = [
            pltpu.make_async_copy(out.at[j], scores_hbm.at[:, across(j)], sems.at[2, j])
            for j in range(blocks)
        ]
        load_rows.start()
        for j in range(blocks):
            load_vocab[j].start()
            load_wanted[j].start()
        load_rows.wait()
        top = jnp.full((tokens, LANES), -jnp.inf, F32)
        total = jnp.zeros((tokens, LANES), F32)
        target = jnp.zeros((tokens, LANES), F32)
        for j in range(blocks):
            load_vocab[j].wait()
            out[j] = (
                jnp.dot(rows_in[...], vocab_in[j], preferred_element_type=F32)
                + bias_ref[:, j * SCORE_BLOCK : (j + 1) * SCORE_BLOCK]
            )
            store[j].start()
            load_wanted[j].wait()
            parts = [out[j, :, at : at + LANES] for at in range(0, SCORE_BLOCK, LANES)]
            new_top = top
            for part in parts:
                new_top = jnp.maximum(new_top, part)
            total = total * jnp.exp(top - new_top)
            for at, part in enumerate(parts):
                total = total + jnp.exp(part - new_top)
                target = target + wanted_in[j, :, at * LANES : (at + 1) * LANES] * part
            top = new_top
        row_top = jnp.max(top, axis=1, keepdims=True)
        row_total = jnp.sum(total * jnp.exp(top - row_top), axis=1, keepdims=True)
        row_target = jnp.sum(target, axis=1, keepdims=True)
        lane = lax.broadcasted_iota(jnp.int32, (tokens, LANES), 1)
        packed = jnp.where(lane == 0, row_top, jnp.where(lane == 1, row_total, row_target))
        stats_ref[...] = packed.T[:8]
        for copy in store:
            copy.wait()

    scores, stats = call(
        kernel,
        (1,),
        [HBM, HBM, pl.BlockSpec((1, columns), lambda i: (0, 0)), HBM],
        [HBM, pl.BlockSpec((8, tokens), lambda i: (0, 0))],
        [
            jax.ShapeDtypeStruct((tokens, columns), F32),
            jax.ShapeDtypeStruct((8, tokens), F32),
        ],
        [rows, vocab, bias.reshape(1, columns), wanted],
        2 * tokens * width * columns,
        scratch=[
            pltpu.VMEM((tokens, width), BF16),
            pltpu.VMEM((blocks, width, SCORE_BLOCK), BF16),
            pltpu.VMEM((blocks, tokens, SCORE_BLOCK), F32),
            pltpu.VMEM((blocks, tokens, SCORE_BLOCK), F32),
            pltpu.SemaphoreType.DMA((4, blocks)),
        ],
    )
    return scores, stats[:3]


def gradients(scores, log_norm, wanted, rows, index, lists, chunk):
    tokens, columns = scores.shape
    width = rows.shape[0]
    half = columns // 2
    part = 128
    steps = tokens // part
    tall = 512
    count = sum(len(some) for some in lists)

    def kernel(index_ref, scores_hbm, norm_ref, wanted_hbm, rows_hbm, grads_hbm, *refs):
        outs = refs[: len(lists)]
        scores_in, wanted_in, rows_in, kept, product, load_sems, store_sems, out_sems = refs[len(lists) :]

        def down(i):
            return pl.ds(i * part, part)

        load_scores = [
            pltpu.make_async_copy(scores_hbm.at[down(i)], scores_in.at[down(i)], load_sems.at[0, i])
            for i in range(steps)
        ]
        load_wanted = [
            pltpu.make_async_copy(wanted_hbm.at[down(i)], wanted_in.at[down(i)], load_sems.at[1, i])
            for i in range(steps)
        ]
        load_rows = pltpu.make_async_copy(rows_hbm, rows_in, load_sems.at[2, 0])
        for i in range(steps):
            load_scores[i].start()
            load_wanted[i].start()
        load_rows.start()
        store_grads = []
        for i in range(steps):
            load_scores[i].wait()
            load_wanted[i].wait()
            norm = jnp.broadcast_to(norm_ref[i * part : (i + 1) * part], (part, LANES))
            factor = 1.0 + 2.0 * z_weight * norm
            for at in range(0, columns, LANES):
                cell = (slice(i * part, (i + 1) * part), slice(at, at + LANES))
                probability = jnp.exp(scores_in[cell] - norm)
                value = (loss_scale * (probability * factor - wanted_in[cell])).astype(BF16)
                kept[at // half, cell[0], at % half : at % half + LANES] = value
            for side in (0, 1):
                store_grads.append(
                    pltpu.make_async_copy(
                        kept.at[side, down(i)],
                        grads_hbm.at[down(i), pl.ds(side * half, half)],
                        store_sems.at[side, i],
                    )
                )
                store_grads[-1].start()
        load_rows.wait()
        store_blocks = []
        for slot in (0, 1):
            side = index_ref[0] if slot == 0 else 1 - index_ref[0]
            for at in range(0, width, tall):
                product[slot, at : at + tall] = jnp.dot(
                    rows_in[at : at + tall], kept[side], preferred_element_type=F32
                ).astype(BF16)
            flat = 0
            for out, some in zip(outs, lists):
                for k, (place, its_slot) in enumerate(some):
                    if its_slot == slot:
                        start = pl.multiple_of(index_ref[place] * chunk, chunk)
                        store_blocks.append(
                            pltpu.make_async_copy(
                                product.at[slot, pl.ds(start, chunk)], out.at[k], out_sems.at[flat]
                            )
                        )
                        store_blocks[-1].start()
                    flat += 1
        for copy in store_grads + store_blocks:
            copy.wait()

    results = call(
        kernel,
        (1,),
        [HBM, pl.BlockSpec((tokens, 1), lambda i, idx: (0, 0)), HBM, HBM],
        [HBM] * (1 + len(lists)),
        [jax.ShapeDtypeStruct(scores.shape, BF16)]
        + [jax.ShapeDtypeStruct((len(some), chunk, half), BF16) for some in lists],
        [scores, log_norm[:, None], wanted, rows],
        2 * width * columns * tokens,
        scratch=[
            pltpu.VMEM((tokens, columns), F32),
            pltpu.VMEM((tokens, columns), F32),
            pltpu.VMEM(rows.shape, BF16),
            pltpu.VMEM((2, tokens, half), BF16),
            pltpu.VMEM((2, width, half), BF16),
            pltpu.SemaphoreType.DMA((3, steps)),
            pltpu.SemaphoreType.DMA((2, steps)),
            pltpu.SemaphoreType.DMA((count,)),
        ],
        scalars=index,
    )
    return results[0], results[1:]


def row_gradients(grads, vocab):
    tokens, columns = grads.shape
    width = vocab.shape[0]
    blocks = 4
    rows = width // blocks

    def kernel(grads_hbm, vocab_hbm, out_hbm, grads_in, vocab_in, out, sems):
        load_grads = pltpu.make_async_copy(grads_hbm, grads_in, sems.at[2, 0])
        load_vocab = [
            pltpu.make_async_copy(vocab_hbm.at[pl.ds(j * rows, rows)], vocab_in.at[j], sems.at[0, j])
            for j in range(blocks)
        ]
        store = [
            pltpu.make_async_copy(out.at[j], out_hbm.at[:, pl.ds(j * rows, rows)], sems.at[1, j])
            for j in range(blocks)
        ]
        load_grads.start()
        for copy in load_vocab:
            copy.start()
        load_grads.wait()
        for j in range(blocks):
            load_vocab[j].wait()
            out[j] = lax.dot_general(
                grads_in[...], vocab_in[j], (((1,), (1,)), ((), ())), preferred_element_type=F32
            ).astype(BF16)
            store[j].start()
        for copy in store:
            copy.wait()

    return call(
        kernel,
        (1,),
        [HBM, HBM],
        HBM,
        jax.ShapeDtypeStruct((tokens, width), BF16),
        [grads, vocab],
        2 * tokens * columns * width,
        scratch=[
            pltpu.VMEM((tokens, columns), BF16),
            pltpu.VMEM((blocks, rows, columns), BF16),
            pltpu.VMEM((blocks, tokens, rows), BF16),
            pltpu.SemaphoreType.DMA((3, blocks)),
        ],
    )


def shards(
    hidden_act,
    down_weight,
    residual,
    post_gain,
    final_gain,
    vocab,
    vocab_bias,
    target_ids,
    target_weights,
):
    own_rows = residual.shape[0]
    width, columns = vocab.shape
    vp_index = lax.axis_index(VP)
    z_index = lax.axis_index("z")
    core = lax.axis_index("c")
    n_z = lax.axis_size("z")

    branch_parts = jnp.dot(hidden_act, down_weight, preferred_element_type=F32).astype(BF16)
    branch = summed_over(branch_parts, VP)
    stream = residual.astype(F32) + branch * inverse_rms(branch) * post_gain
    inverse = inverse_rms(stream)
    normed = (stream * inverse * final_gain).astype(BF16)

    gathered = copied_over(normed, VP)
    ids = target_ids - vp_index * columns
    wanted = wanted_matrix(ids, target_weights, columns, (branch_parts,))
    scores, stats = scored(gathered, vocab, vocab_bias, wanted)
    normed_rows = turned(gathered, (stats,))
    n_vp = lax.axis_size(VP)
    stats = exchange(jnp.broadcast_to(stats, (n_vp, *stats.shape)), VP)
    row_max = jnp.max(stats[:, 0], axis=0)
    row_sum = jnp.sum(stats[:, 1] * jnp.exp(stats[:, 0] - row_max), axis=0)
    target_score = jnp.sum(stats[:, 2], axis=0)
    log_norm = row_max + jnp.log(row_sum)
    group_losses = log_norm - target_score + z_weight * log_norm * log_norm
    losses = lax.dynamic_slice_in_dim(group_losses, vp_index * own_rows, own_rows)
    chunk = width // n_z
    far = n_z // 2
    way = 1 - 2 * core

    def swapped(x):
        return lax.ppermute(x, "c", [(0, 1), (1, 0)])

    ring = [
        (z * 2 + c, (z + (1, -1)[c]) % n_z * 2 + c) for z in range(n_z) for c in (0, 1)
    ]

    def sent(x):
        return lax.ppermute(x.astype(BF16), DP, ring)

    index = jnp.stack(
        [1 - core]
        + [(z_index + way * d + n_z) % n_z for d in range(far + 1)]
        + [(z_index - way * d + n_z) % n_z for d in range(far + 1)]
    )

    def own_block(distance, lane):
        return (1 + distance, 1 - lane)

    def their_block(distance, lane):
        return (2 + far + distance, lane)

    first = [(far, 0), (far - 1, 1), (far - 1, 0)]
    rest = [(d, lane) for d in range(far - 2, 0, -1) for lane in (1, 0)]
    owned = first + rest + [(0, 0), (0, 1)]
    grads, products = gradients(
        scores,
        log_norm,
        wanted,
        normed_rows,
        index,
        [[their_block(*key) for key in first]]
        + [[their_block(*key)] for key in rest]
        + [[own_block(*key)] for key in owned],
        chunk,
    )
    passed_first = swapped(products[0])
    passed = {key: passed_first[at] for at, key in enumerate(first)}
    passed.update({key: swapped(block)[0] for key, block in zip(rest, products[1:])})
    own = {key: block[0] for key, block in zip(owned, products[1 + len(rest) :])}

    def message(key, *carried):
        return sum(x.astype(F32) for x in (own[key], passed[key], *carried)).astype(BF16)

    carried = [sent(message((far, 0))), sent(message((far - 1, 1)))]
    for distance in range(far - 1, 0, -1):
        for lane, key in ((0, (distance, 0)), (1, (distance - 1, 1))):
            if key in owned and key[0] > 0:
                carried[lane] = sent(message(key, carried[lane]))
    slice_rows = chunk // 2
    arrived, passed = [], []
    for lane in (0, 1):
        whole = own[0, lane].astype(F32) + carried[lane].astype(F32)
        arrived.append(lax.dynamic_slice_in_dim(whole, core * slice_rows, slice_rows))
        theirs = lax.dynamic_slice_in_dim(whole, (1 - core) * slice_rows, slice_rows)
        passed.append(swapped(theirs.astype(BF16)).astype(F32))
    lanes = [arrived[0] + passed[1], arrived[1] + passed[0]]
    vocab_grad = jnp.concatenate(
        [jnp.where(core == 0, lanes[0], lanes[1]), jnp.where(core == 0, lanes[1], lanes[0])], axis=1
    )

    row_parts = row_gradients(grads, vocab)
    row_grad = summed_over(row_parts, VP)
    upstream = row_grad * final_gain
    stream_grad = inverse * (
        upstream - stream * inverse * inverse * jnp.mean(upstream * stream, axis=-1, keepdims=True)
    )
    return (losses, stream_grad, vocab_grad)


def solution(mesh):
    split = Mesh(mesh.devices.reshape(4, 4, mesh.shape["dp"] // 2, 2), ("y", "x", "z", "c"))
    placed = (
        P(DP, VP),
        P(VP, None),
        P(DP_VP, None),
        P(),
        P(),
        P(None, VP),
        P(VP),
        P(DP, None),
        P(DP, None),
    )

    return jax.shard_map(
        shards,
        mesh=split,
        in_specs=placed,
        out_specs=(P(DP_VP), P(DP_VP, None), P(DP, VP)),
        check_vma=False,
    )
```

profile of v0, /device:TPU:24, one launch (start us, length us, event | category | flops | bytes accessed | tf_op | source)
XLA Modules:
  0.0 188.9 jit_solution(10869290052876707709)
XLA Ops:
  2.2 2.3 %convolution_convert_fusion.refs_2_ = bf16[512,2048]{1,0:T(8,128)(2,1)S(1)} fusion(bf16[512,512]{1,0:T(8,128)(2,1)} %param.9, bf16[512,2048]{1,0:T(8,128)(2,1)S(1)} %copy-done), kind=kOutput, calls=%fused_computation.2 | convolution fusion | flops 1074790400 | bytes 4718592 | tf_op jit(solution)/shard_map/dot_general | solution.py:356
  4.5 33.1 %all_to_all.20 = bf16[16,32,2048]{2,1,0:T(8,128)(2,1)S(1)} all-to-all(bf16[16,32,2048]{2,1,0:T(8,128)(2,1)S(1)} %bitcast.59), channel_id=1, replica_groups=mesh['y'=4,'x'=4,'z'=8,'c'=2] {'y','x'}, dimensions={0} | all-to-all | bytes 4194304 | tf_op jit(solution)/shard_map/all_to_all | solution.py:22
  41.3 6.8 %all-to-all-start.1 = ((bf16[16,32,2048]{2,1,0:T(8,128)(2,1)}), bf16[16,32,2048]{2,1,0:T(8,128)(2,1)}, u32[]{:S(2)}, u32[]{:S(2)}) async-start(bf16[16,32,2048]{2,1,0:T(8,128)(2,1)} %broadcast_in_dim.4), calls=%async_computation.1 | async-start | bytes 4194304 | tf_op jit(solution)/shard_map/all_to_all | solution.py:22
  50.5 5.4 %shard_map.112.refs_3_ = f32[512,2048]{1,0:T(8,128)} custom-call(s32[512,4]{1,0:T(8,128)} %broadcast_subtract_fusion.refs_0_, f32[512,4]{1,0:T(8,128)} %copy.29.refs_1_, bf16[512,2048]{1,0:T(8,128)(2,1)} %copy-done.1), custom_call_target="tpu_custom_call" | custom-call | flops 8388608 | bytes 16384 | tf_op jit(solution)/shard_map/pallas_call | solution.py:49
  55.9 20.1 %all-to-all-done.1 = bf16[16,32,2048]{2,1,0:T(8,128)(2,1)} async-done(((bf16[16,32,2048]{2,1,0:T(8,128)(2,1)}), bf16[16,32,2048]{2,1,0:T(8,128)(2,1)}, u32[]{:S(2)}, u32[]{:S(2)}) %all-to-all-start.1) | async-done | bytes 2097184 | tf_op jit(solution)/shard_map/all_to_all | solution.py:22
  76.0 11.9 %shard_map.113 = (f32[512,2048]{1,0:T(8,128)}, f32[8,512]{1,0:T(8,128)}) custom-call(bf16[512,2048]{1,0:T(8,128)(2,1)} %bitcast.1.refs_0_, bf16[2048,2048]{1,0:T(8,128)(2,1)} %refs_1_.4, f32[1,2048]{1,0:T(1,128)} %bitcast.62, f32[512,2048]{1,0:T(8,128)} %shard_map.112.refs_3_), custom_call_target="tpu_custom_call" | custom-call | flops 4294967296 | bytes 14688256 | tf_op jit(solution)/shard_map/pallas_call | solution.py:49
  89.3 5.2 %all-to-all-start.2 = ((f32[16,3,512]{2,1,0:T(4,128)}), f32[16,3,512]{2,1,0:T(4,128)S(1)}, u32[]{:S(2)}, u32[]{:S(2)}) async-start(f32[16,3,512]{2,1,0:T(4,128)} %broadcast_in_dim.5), calls=%async_computation.2 | async-start | bytes 262144 | tf_op jit(solution)/shard_map/all_to_all | solution.py:22
  94.5 2.9 %shard_map.114.refs_4_ = bf16[2048,512]{1,0:T(8,128)(2,1)} custom-call(bf16[512,2048]{1,0:T(8,128)(2,1)} %bitcast.1.refs_0_, f32[3,512]{1,0:T(4,128)} %copy-done.15), custom_call_target="tpu_custom_call" | custom-call | flops 2097152000 | bytes 2097152 | tf_op jit(solution)/shard_map/pallas_call | solution.py:49
  97.5 2.8 %all-to-all-done.2 = f32[16,3,512]{2,1,0:T(4,128)S(1)} async-done(((f32[16,3,512]{2,1,0:T(4,128)}), f32[16,3,512]{2,1,0:T(4,128)S(1)}, u32[]{:S(2)}, u32[]{:S(2)}) %all-to-all-start.2) | async-done | bytes 98336 | tf_op jit(solution)/shard_map/all_to_all | solution.py:22
  101.8 13.1 %shard_map.115 = (bf16[512,2048]{1,0:T(8,128)(2,1)}, bf16[3,256,1024]{2,1,0:T(8,128)(2,1)}, bf16[1,256,1024]{2,1,0:T(8,128)(2,1)}, bf16[1,256,1024]{2,1,0:T(8,12...) custom-call(s32[11]{0:T(128)} %stack.44.refs_0_, ...), custom_call_target="tpu_custom_call" | custom-call | flops 4294967296 | bytes 10487808 | tf_op jit(solution)/shard_map/pallas_call | solution.py:49
  115.1 8.3 %shard_map.116 = bf16[512,2048]{1,0:T(8,128)(2,1)} custom-call(bf16[512,2048]{1,0:T(8,128)(2,1)} %get-tuple-element.22.refs_0_, bf16[2048,2048]{1,0:T(8,128)(2,1)} %refs_1_.4), custom_call_target="tpu_custom_call" | custom-call | flops 4294967296 | bytes 10485760 | tf_op jit(solution)/shard_map/pallas_call | solution.py:49
  123.5 6.8 %all-to-all-start.3 = ((bf16[16,32,2048]{2,1,0:T(8,128)(2,1)}), bf16[16,32,2048]{2,1,0:T(8,128)(2,1)}, u32[]{:S(2)}, u32[]{:S(2)}) async-start(bf16[16,32,2048]{2,1,0:T(8,128)(2,1)} %bitcast.60), calls=%async_computation.3 | async-start | bytes 4194304 | tf_op jit(solution)/shard_map/all_to_all | solution.py:22
  134.0 3.9 %collective-permute-start.8 = (bf16[1,256,1024]{2,1,0:T(8,128)(2,1)S(1)}, bf16[1,256,1024]{2,1,0:T(8,128)(2,1)S(1)}, u32[]{:S(2)}, u32[]{:S(2)}) collective-permute-start(bf16[1,256,1024]{2,1,0:T(8,128)(2,1)S(1)} %copy-done.22), channel_id=1, source_target_pairs={{0,1},{1,0},{2,3},{3,2},{4,5},{5,4},{6,7},{7,6},{8,9},{9,8},{10,11... | collective-permute-start | bytes 1572872 | tf_op jit(solution)/shard_map/ppermute | solution.py:380
  138.6 6.5 %collective-permute-done.3 = bf16[256,1024]{1,0:T(8,128)(2,1)S(1)} collective-permute-done((bf16[256,1024]{1,0:T(8,128)(2,1)S(1)}, bf16[256,1024]{1,0:T(8,128)(2,1)S(1)}, u32[]{:S(2)}, u32[]{:S(2)}) %collective-permute-start.3) | collective-permute-done | bytes 524320 | tf_op jit(solution)/shard_map/ppermute | solution.py:387
  145.1 2.2 %fusion.2 = bf16[256,1024]{1,0:T(8,128)(2,1)} fusion(bf16[256,1024]{1,0:T(8,128)(2,1)S(1)} %collective-permute-done.3, bf16[1,256,1024]{2,1,0:T(8,128)(2,1)S(1)} %copy-done.10, bf16[3,256,1024]{2,1,0:T(8,128)(2,1)} %collective-permute-done.2), kind=kLoop, calls=%fused_computation.11 | loop fusion | flops 1572864 | bytes 2097152 | tf_op jit(solution)/shard_map/convert_element_type | solution.py:421
  147.3 2.4 %collective-permute-start.7 = (bf16[1,256,1024]{2,1,0:T(8,128)(2,1)}, bf16[1,256,1024]{2,1,0:T(8,128)(2,1)}, u32[]{:S(2)}, u32[]{:S(2)}) collective-permute-start(bf16[1,256,1024]{2,1,0:T(8,128)(2,1)} %get-tuple-element.33), channel_id=1, source_target_pairs={{0,1},{1,0},{2,3},{3,2},{4,5},{5,4},{6,7},{7,6},{8,9},{9,8},{10,11... | collective-permute-start | bytes 1572872 | tf_op jit(solution)/shard_map/ppermute | solution.py:380
  151.8 2.4 %collective-permute-start = (bf16[1,256,1024]{2,1,0:T(8,128)(2,1)}, bf16[1,256,1024]{2,1,0:T(8,128)(2,1)}, u32[]{:S(2)}, u32[]{:S(2)}) collective-permute-start(bf16[1,256,1024]{2,1,0:T(8,128)(2,1)} %get-tuple-element.25), channel_id=1, source_target_pairs={{0,1},{1,0},{2,3},{3,2},{4,5},{5,4},{6,7},{7,6},{8,9},{9,8},{10,11... | collective-permute-start | bytes 1572872 | tf_op jit(solution)/shard_map/ppermute | solution.py:380
  155.5 2.5 %collective-permute-done.4 = bf16[256,1024]{1,0:T(8,128)(2,1)} collective-permute-done((bf16[256,1024]{1,0:T(8,128)(2,1)}, bf16[256,1024]{1,0:T(8,128)(2,1)}, u32[]{:S(2)}, u32[]{:S(2)}) %collective-permute-start.4) | collective-permute-done | bytes 524320 | tf_op jit(solution)/shard_map/ppermute | solution.py:387
  158.0 2.3 %fusion.3 = bf16[256,1024]{1,0:T(8,128)(2,1)} fusion(bf16[256,1024]{1,0:T(8,128)(2,1)} %collective-permute-done.4, bf16[1,256,1024]{2,1,0:T(8,128)(2,1)} %copy-done.8, bf16[1,256,1024]{2,1,0:T(8,128)(2,1)S(1)} %copy-done.7), kind=kLoop, calls=%fused_computation.13 | loop fusion | flops 1572864 | bytes 2097152 | tf_op jit(solution)/shard_map/convert_element_type | solution.py:421
  160.3 3.1 %all-to-all-done.3 = bf16[16,32,2048]{2,1,0:T(8,128)(2,1)} async-done(((bf16[16,32,2048]{2,1,0:T(8,128)(2,1)}), bf16[16,32,2048]{2,1,0:T(8,128)(2,1)}, u32[]{:S(2)}, u32[]{:S(2)}) %all-to-all-start.3) | async-done | bytes 2097184 | tf_op jit(solution)/shard_map/all_to_all | solution.py:22
  163.5 2.0 %convert_reduce_fusion = f32[32,2048]{1,0:T(8,128)S(1)} fusion(bf16[16,32,2048]{2,1,0:T(8,128)(2,1)} %all-to-all-done.3), kind=kLoop, calls=%fused_computation | loop fusion | flops 2031616 | bytes 2359296 | tf_op jit(solution)/shard_map/reduce_sum | solution.py:28
  167.1 2.0 %collective-permute-start.11 = (bf16[256,1024]{1,0:T(8,128)(2,1)S(1)}, bf16[256,1024]{1,0:T(8,128)(2,1)S(1)}, u32[]{:S(2)}, u32[]{:S(2)}) collective-permute-start(bf16[256,1024]{1,0:T(8,128)(2,1)S(1)} %fusion.1), channel_id=1, source_target_pairs={{0,2},{1,15},{2,4},{3,1},{4,6},{5,3},{6,8},{7,5},{8,10},{9,7},{10,... | collective-permute-start | bytes 1572872 | tf_op jit(solution)/shard_map/ppermute | solution.py:387
  172.8 7.3 %collective-permute-done.11 = bf16[256,1024]{1,0:T(8,128)(2,1)S(1)} collective-permute-done((bf16[256,1024]{1,0:T(8,128)(2,1)S(1)}, bf16[256,1024]{1,0:T(8,128)(2,1)S(1)}, u32[]{:S(2)}, u32[]{:S(2)}) %collective-permute-start.11) | collective-permute-done | bytes 524320 | tf_op jit(solution)/shard_map/ppermute | solution.py:387
  180.5 5.3 %collective-permute-done.6 = bf16[256,1024]{1,0:T(8,128)(2,1)S(1)} collective-permute-done((bf16[256,1024]{1,0:T(8,128)(2,1)S(1)}, bf16[256,1024]{1,0:T(8,128)(2,1)S(1)}, u32[]{:S(2)}, u32[]{:S(2)}) %collective-permute-start.6) | collective-permute-done | bytes 524320 | tf_op jit(solution)/shard_map/ppermute | solution.py:387
  (97 shorter events, 27.3 us)
Async XLA Ops:
  4.5 33.1 %copy-start.1 = (bf16[512,2048]{1,0:T(8,128)(2,1)}, bf16[512,2048]{1,0:T(8,128)(2,1)S(1)}, u32[]{:S(2)}) copy-start(bf16[512,2048]{1,0:T(8,128)(2,1)S(1)} %convolution_convert_fusion.refs_2_) | copy-start | bytes 6291460
  41.3 34.7 %all-to-all-start.1 = ((bf16[16,32,2048]{2,1,0:T(8,128)(2,1)}), bf16[16,32,2048]{2,1,0:T(8,128)(2,1)}, u32[]{:S(2)}, u32[]{:S(2)}) async-start(bf16[16,32,2048]{2,1,0:T(8,128)(2,1)} %broadcast_in_dim.4), calls=%async_computation.1 | async-start | bytes 4194304 | tf_op jit(solution)/shard_map/all_to_all | solution.py:22
  89.3 10.9 %all-to-all-start.2 = ((f32[16,3,512]{2,1,0:T(4,128)}), f32[16,3,512]{2,1,0:T(4,128)S(1)}, u32[]{:S(2)}, u32[]{:S(2)}) async-start(f32[16,3,512]{2,1,0:T(4,128)} %broadcast_in_dim.5), calls=%async_computation.2 | async-start | bytes 262144 | tf_op jit(solution)/shard_map/all_to_all | solution.py:22
  115.0 15.3 %collective-permute-start.2 = (bf16[3,256,1024]{2,1,0:T(8,128)(2,1)}, bf16[3,256,1024]{2,1,0:T(8,128)(2,1)}, u32[]{:S(2)}, u32[]{:S(2)}) collective-permute-start(bf16[3,256,1024]{2,1,0:T(8,128)(2,1)} %get-tuple-element.29), channel_id=1, source_target_pairs={{0,1},{1,0},{2,3},{3,2},{4,5},{5,4},{6,7},{7,6},{8,9},{9,8},{10,11... | collective-permute-start | bytes 4718600 | tf_op jit(solution)/shard_map/ppermute | solution.py:380
  123.5 40.0 %all-to-all-start.3 = ((bf16[16,32,2048]{2,1,0:T(8,128)(2,1)}), bf16[16,32,2048]{2,1,0:T(8,128)(2,1)}, u32[]{:S(2)}, u32[]{:S(2)}) async-start(bf16[16,32,2048]{2,1,0:T(8,128)(2,1)} %bitcast.60), calls=%async_computation.3 | async-start | bytes 4194304 | tf_op jit(solution)/shard_map/all_to_all | solution.py:22
  130.2 14.9 %copy-start.10 = (bf16[1,256,1024]{2,1,0:T(8,128)(2,1)S(1)}, bf16[1,256,1024]{2,1,0:T(8,128)(2,1)}, u32[]{:S(2)}) copy-start(bf16[1,256,1024]{2,1,0:T(8,128)(2,1)} %get-tuple-element.28) | copy-start | bytes 1572868
  130.3 20.4 %copy-start.9 = (bf16[1,256,1024]{2,1,0:T(8,128)(2,1)S(1)}, bf16[1,256,1024]{2,1,0:T(8,128)(2,1)}, u32[]{:S(2)}) copy-start(bf16[1,256,1024]{2,1,0:T(8,128)(2,1)} %get-tuple-element.34) | copy-start | bytes 1572868
  132.0 13.1 %collective-permute-start.3 = (bf16[256,1024]{1,0:T(8,128)(2,1)S(1)}, bf16[256,1024]{1,0:T(8,128)(2,1)S(1)}, u32[]{:S(2)}, u32[]{:S(2)}) collective-permute-start(bf16[256,1024]{1,0:T(8,128)(2,1)S(1)} %get-tuple-element.43), channel_id=1, source_target_pairs={{0,2},{1,15},{2,4},{3,1},{4,6},{5,3},{6,8},{7,5},{8,10},{9,7},{10,... | collective-permute-start | bytes 1572872 | tf_op jit(solution)/shard_map/ppermute | solution.py:387
  134.0 15.7 %collective-permute-start.8 = (bf16[1,256,1024]{2,1,0:T(8,128)(2,1)S(1)}, bf16[1,256,1024]{2,1,0:T(8,128)(2,1)S(1)}, u32[]{:S(2)}, u32[]{:S(2)}) collective-permute-start(bf16[1,256,1024]{2,1,0:T(8,128)(2,1)S(1)} %copy-done.22), channel_id=1, source_target_pairs={{0,1},{1,0},{2,3},{3,2},{4,5},{5,4},{6,7},{7,6},{8,9},{9,8},{10,11... | collective-permute-start | bytes 1572872 | tf_op jit(solution)/shard_map/ppermute | solution.py:380
  137.9 12.8 %collective-permute-start.9 = (bf16[256,1024]{1,0:T(8,128)(2,1)S(1)}, bf16[256,1024]{1,0:T(8,128)(2,1)S(1)}, u32[]{:S(2)}, u32[]{:S(2)}) collective-permute-start(bf16[256,1024]{1,0:T(8,128)(2,1)S(1)} %get-tuple-element.44), channel_id=1, source_target_pairs={{0,2},{1,15},{2,4},{3,1},{4,6},{5,3},{6,8},{7,5},{8,10},{9,7},{10,... | collective-permute-start | bytes 1572872 | tf_op jit(solution)/shard_map/ppermute | solution.py:387
  137.9 17.6 %collective-permute-start.1 = (bf16[1,256,1024]{2,1,0:T(8,128)(2,1)}, bf16[1,256,1024]{2,1,0:T(8,128)(2,1)S(1)}, u32[]{:S(2)}, u32[]{:S(2)}) collective-permute-start(bf16[1,256,1024]{2,1,0:T(8,128)(2,1)} %get-tuple-element.27), channel_id=1, source_target_pairs={{0,1},{1,0},{2,3},{3,2},{4,5},{5,4},{6,7},{7,6},{8,9},{9,8},{10,11... | collective-permute-start | bytes 1572872 | tf_op jit(solution)/shard_map/ppermute | solution.py:380
  145.1 12.9 %copy-start.7 = (bf16[1,256,1024]{2,1,0:T(8,128)(2,1)S(1)}, bf16[1,256,1024]{2,1,0:T(8,128)(2,1)}, u32[]{:S(2)}) copy-start(bf16[1,256,1024]{2,1,0:T(8,128)(2,1)} %get-tuple-element.26) | copy-start | bytes 1572868
  147.3 10.7 %collective-permute-start.4 = (bf16[256,1024]{1,0:T(8,128)(2,1)}, bf16[256,1024]{1,0:T(8,128)(2,1)}, u32[]{:S(2)}, u32[]{:S(2)}) collective-permute-start(bf16[256,1024]{1,0:T(8,128)(2,1)} %fusion.2), channel_id=1, source_target_pairs={{0,2},{1,15},{2,4},{3,1},{4,6},{5,3},{6,8},{7,5},{8,10},{9,7},{10,... | collective-permute-start | bytes 1572872 | tf_op jit(solution)/shard_map/ppermute | solution.py:387
  147.3 18.2 %collective-permute-start.7 = (bf16[1,256,1024]{2,1,0:T(8,128)(2,1)}, bf16[1,256,1024]{2,1,0:T(8,128)(2,1)}, u32[]{:S(2)}, u32[]{:S(2)}) collective-permute-start(bf16[1,256,1024]{2,1,0:T(8,128)(2,1)} %get-tuple-element.33), channel_id=1, source_target_pairs={{0,1},{1,0},{2,3},{3,2},{4,5},{5,4},{6,7},{7,6},{8,9},{9,8},{10,11... | collective-permute-start | bytes 1572872 | tf_op jit(solution)/shard_map/ppermute | solution.py:380
  151.8 13.7 %collective-permute-start.10 = (bf16[256,1024]{1,0:T(8,128)(2,1)}, bf16[256,1024]{1,0:T(8,128)(2,1)}, u32[]{:S(2)}, u32[]{:S(2)}) collective-permute-start(bf16[256,1024]{1,0:T(8,128)(2,1)} %fusion), channel_id=1, source_target_pairs={{0,2},{1,15},{2,4},{3,1},{4,6},{5,3},{6,8},{7,5},{8,10},{9,7},{10,... | collective-permute-start | bytes 1572872 | tf_op jit(solution)/shard_map/ppermute | solution.py:387
  151.8 17.5 %collective-permute-start = (bf16[1,256,1024]{2,1,0:T(8,128)(2,1)}, bf16[1,256,1024]{2,1,0:T(8,128)(2,1)}, u32[]{:S(2)}, u32[]{:S(2)}) collective-permute-start(bf16[1,256,1024]{2,1,0:T(8,128)(2,1)} %get-tuple-element.25), channel_id=1, source_target_pairs={{0,1},{1,0},{2,3},{3,2},{4,5},{5,4},{6,7},{7,6},{8,9},{9,8},{10,11... | collective-permute-start | bytes 1572872 | tf_op jit(solution)/shard_map/ppermute | solution.py:380
  160.3 10.7 %copy-start.5 = (bf16[1,256,1024]{2,1,0:T(8,128)(2,1)S(1)}, bf16[1,256,1024]{2,1,0:T(8,128)(2,1)}, u32[]{:S(2)}) copy-start(bf16[1,256,1024]{2,1,0:T(8,128)(2,1)} %get-tuple-element.24) | copy-start | bytes 1572868
  160.3 10.7 %collective-permute-start.5 = (bf16[256,1024]{1,0:T(8,128)(2,1)}, bf16[256,1024]{1,0:T(8,128)(2,1)}, u32[]{:S(2)}, u32[]{:S(2)}) collective-permute-start(bf16[256,1024]{1,0:T(8,128)(2,1)} %fusion.3), channel_id=1, source_target_pairs={{0,2},{1,15},{2,4},{3,1},{4,6},{5,3},{6,8},{7,5},{8,10},{9,7},{10,... | collective-permute-start | bytes 1572872 | tf_op jit(solution)/shard_map/ppermute | solution.py:387
  165.5 14.6 %copy-start.4 = (bf16[1,256,1024]{2,1,0:T(8,128)(2,1)S(1)}, bf16[1,256,1024]{2,1,0:T(8,128)(2,1)}, u32[]{:S(2)}) copy-start(bf16[1,256,1024]{2,1,0:T(8,128)(2,1)} %get-tuple-element.31) | copy-start | bytes 1572868
  167.1 13.1 %collective-permute-start.11 = (bf16[256,1024]{1,0:T(8,128)(2,1)S(1)}, bf16[256,1024]{1,0:T(8,128)(2,1)S(1)}, u32[]{:S(2)}, u32[]{:S(2)}) collective-permute-start(bf16[256,1024]{1,0:T(8,128)(2,1)S(1)} %fusion.1), channel_id=1, source_target_pairs={{0,2},{1,15},{2,4},{3,1},{4,6},{5,3},{6,8},{7,5},{8,10},{9,7},{10,... | collective-permute-start | bytes 1572872 | tf_op jit(solution)/shard_map/ppermute | solution.py:387
  171.0 14.7 %copy-start.3 = (bf16[1,256,1024]{2,1,0:T(8,128)(2,1)S(1)}, bf16[1,256,1024]{2,1,0:T(8,128)(2,1)}, u32[]{:S(2)}) copy-start(bf16[1,256,1024]{2,1,0:T(8,128)(2,1)} %get-tuple-element.23) | copy-start | bytes 1572868
  172.6 13.2 %collective-permute-start.6 = (bf16[256,1024]{1,0:T(8,128)(2,1)S(1)}, bf16[256,1024]{1,0:T(8,128)(2,1)S(1)}, u32[]{:S(2)}, u32[]{:S(2)}) collective-permute-start(bf16[256,1024]{1,0:T(8,128)(2,1)S(1)} %fusion.4), channel_id=1, source_target_pairs={{0,2},{1,15},{2,4},{3,1},{4,6},{5,3},{6,8},{7,5},{8,10},{9,7},{10,... | collective-permute-start | bytes 1572872 | tf_op jit(solution)/shard_map/ppermute | solution.py:387
  180.4 6.6 %collective-permute-start.12 = (bf16[128,1024]{1,0:T(8,128)(2,1)S(1)}, bf16[128,1024]{1,0:T(8,128)(2,1)S(1)}, u32[]{:S(2)}, u32[]{:S(2)}) collective-permute-start(bf16[128,1024]{1,0:T(8,128)(2,1)S(1)} %dynamic-slice_convert_fusion.1), channel_id=1, source_target_pairs={{0,1},{1,0},{2,3},{3,2},{4,5},{5,4},{6,7},{7,6},{8,9},{9,8},{10,11... | collective-permute-start | bytes 786440 | tf_op jit(solution)/shard_map/ppermute | solution.py:380
  186.0 1.6 collective-permute-start.13
  (16 other events, 64.7 us)
where the time goes:
time: 192 us; the launch traced here: 189 us
  waiting for transfers between devices  51.1 us (27%)
  Pallas kernels  41.7 us (22%)
  blocking collectives  33.1 us (17%)
  starting transfers between devices  32.7 us (17%)
  other arithmetic  17.3 us (9%)
  local copies, waits for them, and re-layouts  9.76 us (5%)
  matrix products  2.3 us (1%)
    pallas_call x5, Pallas kernels, call(): pl.pallas_call(body, grid_spec=pltpu.PrefetchScalarGridSpec(num_scalar_pr...  41.7 us
    all_to_all x1, blocking collectives, exchange(): return lax.all_to_all(parts, axis, split_axis=0, concat_axis=0, tiled=True)  33.1 us
    all_to_all x3, waiting for transfers between devices, exchange(): return lax.all_to_all(parts, axis, split_axis=0, concat_axis=0, tiled=True)  26 us
    ppermute x7, waiting for transfers between devices, sent(): return lax.ppermute(x.astype(BF16), DP, ring)  24.4 us
    all_to_all x3, starting transfers between devices, exchange(): return lax.all_to_all(parts, axis, split_axis=0, concat_axis=0, tiled=True)  18.7 us
    convert_element_type x6, other arithmetic, message(): sum((x.astype(F32) for x in (own[key], passed[key], *carried))).astype(BF16)  10.3 us
    ppermute x7, starting transfers between devices, swapped(): return lax.ppermute(x, 'c', [(0, 1), (1, 0)])  9.73 us
    ppermute x7, starting transfers between devices, sent(): return lax.ppermute(x.astype(BF16), DP, ring)  4.24 us
  transfers between devices with their start and end apart: 17, of which 10 were waited for; matrix products, arithmetic and copies ran while one was open for 9% of the time, Pallas kernels for 9%

commit v1 on v0

v1 whole, which is shorter than its diff:
```python
import jax
import jax.numpy as jnp
from jax import lax
from jax.experimental import pallas as pl
from jax.experimental.pallas import tpu as pltpu
from jax.sharding import Mesh
from jax.sharding import PartitionSpec as P


F32 = jnp.float32
BF16 = jnp.bfloat16
VP = ("y", "x")
DP = ("z", "c")
DP_VP = ("z", "c", "y", "x")

epsilon = 1e-06
z_weight = 0.001
loss_scale = 32.0


def exchange(parts, axis):
    return lax.all_to_all(parts, axis, split_axis=0, concat_axis=0, tiled=True)


def summed_over(rows, axis):
    size = lax.axis_size(axis)
    parts = rows.astype(BF16).reshape(size, rows.shape[0] // size, rows.shape[1])
    return jnp.sum(exchange(parts, axis).astype(F32), axis=0)


def copied_over(rows, axis):
    size = lax.axis_size(axis)
    copies = jnp.broadcast_to(rows, (size, *rows.shape))
    return exchange(copies, axis).reshape(size * rows.shape[0], rows.shape[1])


def inverse_rms(values):
    return lax.rsqrt(jnp.mean(values * values, axis=-1, keepdims=True) + epsilon)


def call(kernel, grid, in_specs, out_specs, out_shape, operands, flops, after=(), scratch=(), scalars=None, aliases={}, vmem=16):
    lead = 0 if scalars is None else 1
    used = len(operands)

    def body(*refs):
        kernel(*refs[: lead + used], *refs[lead + used + len(after) :])

    moved = sum(x.size * x.dtype.itemsize for x in operands)
    return pl.pallas_call(
        body,
        grid_spec=pltpu.PrefetchScalarGridSpec(
            num_scalar_prefetch=lead,
            grid=grid,
            in_specs=list(in_specs) + [pl.BlockSpec(memory_space=pl.ANY)] * len(after),
            out_specs=out_specs,
            scratch_shapes=scratch,
        ),
        out_shape=out_shape,
        input_output_aliases=aliases,
        compiler_params=pltpu.CompilerParams(vmem_limit_bytes=vmem << 20),
        cost_estimate=pl.CostEstimate(flops=flops, bytes_accessed=moved, transcendentals=0),
    )(*(() if scalars is None else (scalars,)), *operands, *after)


LANES = 128
SCORE_BLOCK = 512
HBM = pl.BlockSpec(memory_space=pltpu.HBM)
NEAR = pl.BlockSpec(memory_space=pltpu.VMEM)


def wanted_matrix(ids, weights, columns, after):
    tokens = ids.shape[0]
    rows = 128

    def kernel(ids_ref, weights_ref, out_ref):
        wide = (rows, LANES)
        at_ids = [jnp.broadcast_to(ids_ref[:, k : k + 1], wide) for k in range(ids.shape[1])]
        at_weights = [jnp.broadcast_to(weights_ref[:, k : k + 1], wide) for k in range(ids.shape[1])]
        lane = lax.broadcasted_iota(jnp.int32, wide, 1)
        for at in range(0, columns, LANES):
            found = jnp.zeros(wide, F32)
            for k in range(ids.shape[1]):
                found = found + jnp.where(at_ids[k] == lane + at, at_weights[k], 0.0)
            out_ref[:, at : at + LANES] = found

    def block(shape):
        return pl.BlockSpec((rows, shape[1]), lambda i: (i, 0))

    return call(
        kernel,
        (tokens // rows,),
        [block(ids.shape), block(weights.shape)],
        block((tokens, columns)),
        jax.ShapeDtypeStruct((tokens, columns), F32),
        [ids, weights],
        8 * tokens * columns,
        after,
    )


def scored(rows, vocab, bias, wanted):
    tokens, width = rows.shape
    columns = vocab.shape[1]
    blocks = [slice(at, at + SCORE_BLOCK) for at in range(0, columns, SCORE_BLOCK)]

    def kernel(rows_ref, vocab_hbm, bias_ref, wanted_hbm, out_ref, stats_ref, vocab_ref, wanted_ref, turned_ref, sems):
        deep = width // 4
        load_vocab = [
            pltpu.make_async_copy(
                vocab_hbm.at[pl.ds(i * deep, deep)], vocab_ref.at[pl.ds(i * deep, deep)], sems.at[i]
            )
            for i in range(4)
        ]
        load_wanted = pltpu.make_async_copy(wanted_hbm, wanted_ref, sems.at[4])
        near, rest = slice(0, 2 * deep), slice(2 * deep, width)
        load_vocab[0].start()
        load_vocab[1].start()
        load_vocab[0].wait()
        load_vocab[2].start()
        load_vocab[1].wait()
        load_vocab[3].start()
        load_wanted.start()
        turn = width // len(blocks)
        for j, across in enumerate(blocks):
            out_ref[:, across] = jnp.dot(
                rows_ref[:, near], vocab_ref[near, across], preferred_element_type=F32
            )
            turned_ref[j * turn : (j + 1) * turn] = rows_ref[:, j * turn : (j + 1) * turn].T
        top = jnp.full((tokens, LANES), -jnp.inf, F32)
        total = jnp.zeros((tokens, LANES), F32)
        target = jnp.zeros((tokens, LANES), F32)
        load_vocab[2].wait()
        load_vocab[3].wait()
        load_wanted.wait()
        for j in range(len(blocks) + 1):
            if j < len(blocks):
                across = blocks[j]
                out_ref[:, across] = (
                    out_ref[:, across]
                    + jnp.dot(rows_ref[:, rest], vocab_ref[rest, across], preferred_element_type=F32)
                    + bias_ref[:, across]
                )
            if j > 0:
                across = blocks[j - 1]
                lanes = [slice(at, at + LANES) for at in range(across.start, across.stop, LANES)]
                new_top = top
                for at in lanes:
                    new_top = jnp.maximum(new_top, out_ref[:, at])
                total = total * jnp.exp(top - new_top)
                for at in lanes:
                    part = out_ref[:, at]
                    total = total + jnp.exp(part - new_top)
                    target = target + wanted_ref[:, at] * part
                top = new_top
        row_top = jnp.max(top, axis=1, keepdims=True)
        row_total = jnp.sum(total * jnp.exp(top - row_top), axis=1, keepdims=True)
        row_target = jnp.sum(target, axis=1, keepdims=True)
        lane = lax.broadcasted_iota(jnp.int32, (tokens, LANES), 1)
        packed = jnp.where(lane == 0, row_top, jnp.where(lane == 1, row_total, row_target))
        stats_ref[...] = packed.T[:8]

    scores, stats, near_vocab, near_wanted, turned = call(
        kernel,
        (1,),
        [NEAR, HBM, pl.BlockSpec((1, columns), lambda i: (0, 0)), HBM],
        [NEAR, pl.BlockSpec((8, tokens), lambda i: (0, 0)), NEAR, NEAR, NEAR],
        [
            pltpu.VMEM((tokens, columns), F32),
            jax.ShapeDtypeStruct((8, tokens), F32),
            pltpu.VMEM(vocab.shape, vocab.dtype),
            pltpu.VMEM(wanted.shape, wanted.dtype),
            pltpu.VMEM((width, tokens), rows.dtype),
        ],
        [rows, vocab, bias.reshape(1, columns), wanted],
        2 * tokens * width * columns,
        scratch=[pltpu.SemaphoreType.DMA((5,))],
        vmem=42,
    )
    return scores, stats[:3], near_vocab, near_wanted, turned


def gradients(scores, log_norm, wanted, rows, index, lists, chunk):
    tokens, columns = scores.shape
    width = rows.shape[0]
    half = columns // 2
    part = 128

    def kernel(index_ref, scores_ref, norm_ref, wanted_ref, rows_ref, grads_ref, *refs):
        outs, kept = refs[:-1], refs[-1]
        norms = jnp.broadcast_to(norm_ref[...], (LANES, tokens)).T
        for i in range(0, tokens, part):
            norm = norms[i : i + part]
            factor = 1.0 + 2.0 * z_weight * norm
            for at in range(0, columns, LANES):
                cell = (slice(i, i + part), slice(at, at + LANES))
                probability = jnp.exp(scores_ref[cell] - norm)
                value = (loss_scale * (probability * factor - wanted_ref[cell])).astype(BF16)
                grads_ref[cell] = value
                kept[at // half, cell[0], at % half : at % half + LANES] = value
        for out, some in zip(outs, lists):
            for k, (place, slot) in enumerate(some):
                side = index_ref[0] if slot == 0 else 1 - index_ref[0]
                start = pl.multiple_of(index_ref[place] * chunk, chunk)
                out[k] = jnp.dot(
                    rows_ref[pl.ds(start, chunk)], kept[side], preferred_element_type=F32
                ).astype(BF16)

    results = call(
        kernel,
        (1,),
        [NEAR, pl.BlockSpec((1, tokens), lambda i, idx: (0, 0)), NEAR, NEAR],
        [NEAR] * (1 + len(lists)),
        [pltpu.VMEM(scores.shape, BF16)]
        + [pltpu.VMEM((len(some), chunk, half), BF16) for some in lists],
        [scores, log_norm[None], wanted, rows],
        2 * width * columns * tokens,
        scratch=[pltpu.VMEM((2, tokens, half), BF16)],
        scalars=index,
    )
    return results[0], results[1:]


def row_gradients(grads, vocab):
    tokens, columns = grads.shape
    width = vocab.shape[0]

    def kernel(grads_ref, vocab_ref, out_ref):
        for at in range(0, width, 512):
            out_ref[:, at : at + 512] = lax.dot_general(
                grads_ref[...],
                vocab_ref[at : at + 512],
                (((1,), (1,)), ((), ())),
                preferred_element_type=F32,
            ).astype(BF16)

    return call(
        kernel,
        (1,),
        [NEAR, NEAR],
        NEAR,
        pltpu.VMEM((tokens, width), BF16),
        [grads, vocab],
        2 * tokens * columns * width,
    )


def shards(
    hidden_act,
    down_weight,
    residual,
    post_gain,
    final_gain,
    vocab,
    vocab_bias,
    target_ids,
    target_weights,
):
    own_rows = residual.shape[0]
    width, columns = vocab.shape
    vp_index = lax.axis_index(VP)
    z_index = lax.axis_index("z")
    core = lax.axis_index("c")
    n_z = lax.axis_size("z")

    branch_parts = jnp.dot(hidden_act, down_weight, preferred_element_type=F32).astype(BF16)
    branch = summed_over(branch_parts, VP)
    stream = residual.astype(F32) + branch * inverse_rms(branch) * post_gain
    inverse = inverse_rms(stream)
    normed = (stream * inverse * final_gain).astype(BF16)

    gathered = copied_over(normed, VP)
    ids = target_ids - vp_index * columns
    chunk = width // n_z
    far = n_z // 2
    way = 1 - 2 * core
    index = jnp.stack(
        [1 - core]
        + [(z_index + way * d + n_z) % n_z for d in range(far + 1)]
        + [(z_index - way * d + n_z) % n_z for d in range(far + 1)]
    )

    wanted = wanted_matrix(ids, target_weights, columns, (branch_parts, index))
    scores, stats, near_vocab, near_wanted, normed_rows = scored(
        gathered, vocab, vocab_bias, wanted
    )
    n_vp = lax.axis_size(VP)
    stats = exchange(jnp.broadcast_to(stats, (n_vp, *stats.shape)), VP)
    row_max = jnp.max(stats[:, 0], axis=0)
    row_sum = jnp.sum(stats[:, 1] * jnp.exp(stats[:, 0] - row_max), axis=0)
    target_score = jnp.sum(stats[:, 2], axis=0)
    log_norm = row_max + jnp.log(row_sum)
    group_losses = log_norm - target_score + z_weight * log_norm * log_norm
    losses = lax.dynamic_slice_in_dim(group_losses, vp_index * own_rows, own_rows)

    def swapped(x):
        return lax.ppermute(x, "c", [(0, 1), (1, 0)])

    ring = [
        (z * 2 + c, (z + (1, -1)[c]) % n_z * 2 + c) for z in range(n_z) for c in (0, 1)
    ]

    def sent(x):
        return lax.ppermute(x.astype(BF16), DP, ring)

    def own_block(distance, lane):
        return (1 + distance, 1 - lane)

    def their_block(distance, lane):
        return (2 + far + distance, lane)

    first = [(far, 0), (far - 1, 1), (far - 1, 0)]
    rest = [(d, lane) for d in range(far - 2, 0, -1) for lane in (1, 0)]
    owned = first + rest + [(0, 0), (0, 1)]
    grads, products = gradients(
        scores,
        log_norm,
        near_wanted,
        normed_rows,
        index,
        [[their_block(*key) for key in first]]
        + [[their_block(*key)] for key in rest]
        + [[own_block(*key)] for key in owned],
        chunk,
    )
    passed_first = swapped(products[0])
    passed = {key: passed_first[at] for at, key in enumerate(first)}
    passed.update({key: swapped(block)[0] for key, block in zip(rest, products[1:])})
    own = {key: block[0] for key, block in zip(owned, products[1 + len(rest) :])}

    def message(key, *carried):
        return sum(x.astype(F32) for x in (own[key], passed[key], *carried)).astype(BF16)

    carried = [sent(message((far, 0))), sent(message((far - 1, 1)))]
    for distance in range(far - 1, 0, -1):
        for lane, key in ((0, (distance, 0)), (1, (distance - 1, 1))):
            if key in owned and key[0] > 0:
                carried[lane] = sent(message(key, carried[lane]))
    slice_rows = chunk // 2
    arrived, passed = [], []
    for lane in (0, 1):
        for side, parts in ((core, arrived), (1 - core, passed)):
            parts.append(
                sum(
                    lax.dynamic_slice_in_dim(x, side * slice_rows, slice_rows).astype(F32)
                    for x in (own[0, lane], carried[lane])
                )
            )
        passed[lane] = swapped(passed[lane].astype(BF16)).astype(F32)
    lanes = [arrived[0] + passed[1], arrived[1] + passed[0]]
    vocab_grad = jnp.concatenate(
        [jnp.where(core == 0, lanes[0], lanes[1]), jnp.where(core == 0, lanes[1], lanes[0])], axis=1
    )

    row_parts = row_gradients(grads, near_vocab)
    row_grad = summed_over(row_parts, VP)
    upstream = row_grad * final_gain
    stream_grad = inverse * (
        upstream - stream * inverse * inverse * jnp.mean(upstream * stream, axis=-1, keepdims=True)
    )
    return (losses, stream_grad, vocab_grad)


def solution(mesh):
    split = Mesh(mesh.devices.reshape(4, 4, mesh.shape["dp"] // 2, 2), ("y", "x", "z", "c"))
    placed = (
        P(DP, VP),
        P(VP, None),
        P(DP_VP, None),
        P(),
        P(),
        P(None, VP),
        P(VP),
        P(DP, None),
        P(DP, None),
    )

    return jax.shard_map(
        shards,
        mesh=split,
        in_specs=placed,
        out_specs=(P(DP_VP), P(DP_VP, None), P(DP, VP)),
        check_vma=False,
    )
```

time: 192 us -> 175 us (0.911)
  Pallas kernels: 41.7 us -> 26.1 us
  starting transfers between devices: 32.7 us -> 22.6 us
  blocking collectives: 33.1 us -> 43.1 us
    pallas_call x5 -> x4, Pallas kernels: 41.7 us -> 26.1 us  [call(): pl.pallas_call(body, grid_spec=pltpu.PrefetchScalarGridSpec(num_scalar_pr...]
    all_to_all x1 -> x2, blocking collectives: 33.1 us -> 43.1 us  [exchange(): return lax.all_to_all(parts, axis, split_axis=0, concat_axis=0, tiled=True)]
    all_to_all x3 -> x2, starting transfers between devices: 18.7 us -> 13.4 us  [exchange(): return lax.all_to_all(parts, axis, split_axis=0, concat_axis=0, tiled=True)]
    all_to_all x3 -> x2, waiting for transfers between devices: 26 us -> 22.3 us  [exchange(): return lax.all_to_all(parts, axis, split_axis=0, concat_axis=0, tiled=True)]
    ppermute x7, starting transfers between devices: 9.73 us -> 6.15 us  [swapped(): return lax.ppermute(x, 'c', [(0, 1), (1, 0)])]
    ppermute x7, waiting for transfers between devices: 0.67 us -> 3.42 us  [swapped(): return lax.ppermute(x, 'c', [(0, 1), (1, 0)])]
    unnamed x48 -> x40, local copies, waits for them, and re-layouts: 3.85 us -> 6.3 us
  transfers between devices with their start and end apart: 17 -> 16, of which waited for: 10 -> 8; matrix products, arithmetic and copies ran while one was open for 9% -> 7% of each run, Pallas kernels for 9% -> 5%
where the time goes in v1:
time: 175 us; the launch traced here: 173 us
  waiting for transfers between devices  51 us (29%)
  blocking collectives  43.1 us (25%)
  Pallas kernels  26.1 us (15%)
  starting transfers between devices  22.6 us (13%)
  other arithmetic  16.7 us (10%)
  local copies, waits for them, and re-layouts  10 us (6%)
  matrix products  2.3 us (1%)
    all_to_all x2, blocking collectives, exchange(): return lax.all_to_all(parts, axis, split_axis=0, concat_axis=0, tiled=True)  43.1 us
    pallas_call x4, Pallas kernels, call(): pl.pallas_call(body, grid_spec=pltpu.PrefetchScalarGridSpec(num_scalar_pr...  26.1 us
    ppermute x7, waiting for transfers between devices, sent(): return lax.ppermute(x.astype(BF16), DP, ring)  25.2 us
    all_to_all x2, waiting for transfers between devices, exchange(): return lax.all_to_all(parts, axis, split_axis=0, concat_axis=0, tiled=True)  22.3 us
    all_to_all x2, starting transfers between devices, exchange(): return lax.all_to_all(parts, axis, split_axis=0, concat_axis=0, tiled=True)  13.4 us
    convert_element_type x6, other arithmetic, message(): sum((x.astype(F32) for x in (own[key], passed[key], *carried))).astype(BF16)  8.71 us
    unnamed x40, local copies, waits for them, and re-layouts  6.3 us
    ppermute x7, starting transfers between devices, swapped(): return lax.ppermute(x, 'c', [(0, 1), (1, 0)])  6.15 us
  transfers between devices with their start and end apart: 16, of which 8 were waited for; matrix products, arithmetic and copies ran while one was open for 7% of the time, Pallas kernels for 5%

profile of v1, /device:TPU:24, one launch (start us, length us, event | category | flops | bytes accessed | tf_op | source)
XLA Modules:
  0.0 172.9 jit_solution(3027360687976854784)
XLA Ops:
  2.2 2.3 %convolution_convert_fusion.refs_2_ = bf16[512,2048]{1,0:T(8,128)(2,1)S(1)} fusion(bf16[512,512]{1,0:T(8,128)(2,1)} %param.9, bf16[512,2048]{1,0:T(8,128)(2,1)S(1)} %copy-done), kind=kOutput, calls=%fused_computation.2 | convolution fusion | flops 1074790400 | bytes 4718592 | tf_op jit(solution)/shard_map/dot_general | solution.py:265
  4.5 33.1 %all_to_all.20 = bf16[16,32,2048]{2,1,0:T(8,128)(2,1)S(1)} all-to-all(bf16[16,32,2048]{2,1,0:T(8,128)(2,1)S(1)} %bitcast.67), channel_id=1, replica_groups=mesh['y'=4,'x'=4,'z'=8,'c'=2] {'y','x'}, dimensions={0} | all-to-all | bytes 4194304 | tf_op jit(solution)/shard_map/all_to_all | solution.py:22
  41.0 6.8 %all-to-all-start.1 = ((bf16[16,32,2048]{2,1,0:T(8,128)(2,1)}), bf16[16,32,2048]{2,1,0:T(8,128)(2,1)}, u32[]{:S(2)}, u32[]{:S(2)}) async-start(bf16[16,32,2048]{2,1,0:T(8,128)(2,1)} %broadcast_in_dim.4), calls=%async_computation.1 | async-start | bytes 4194304 | tf_op jit(solution)/shard_map/all_to_all | solution.py:22
  48.3 3.1 %shard_map.112.refs_3_ = f32[512,2048]{1,0:T(8,128)S(1)} custom-call(s32[512,4]{1,0:T(8,128)S(1)} %broadcast_subtract_fusion.refs_0_, f32[512,4]{1,0:T(8,128)S(1)} %copy.23.refs_1_, bf16[512,2048]{1,0:T(8,128)(2,1)S(1)} %copy-done.3, s32[11]{0:T(128)S(1)} %stack.44.refs_3_.refs_0_), custom_call_target="tpu_custom_call" | custom-call | flops 8388608 | bytes 16384 | tf_op jit(solution)/shard_map/pallas_call | solution.py:49
  51.4 1.9 %copy-done.4 = f32[512,2048]{1,0:T(8,128)} copy-done((f32[512,2048]{1,0:T(8,128)}, f32[512,2048]{1,0:T(8,128)S(1)}, u32[]{:S(2)}) %copy-start.4) | copy-done | bytes 4194328
  53.3 22.3 %all-to-all-done.1 = bf16[16,32,2048]{2,1,0:T(8,128)(2,1)} async-done(((bf16[16,32,2048]{2,1,0:T(8,128)(2,1)}), bf16[16,32,2048]{2,1,0:T(8,128)(2,1)}, u32[]{:S(2)}, u32[]{:S(2)}) %all-to-all-start.1) | async-done | bytes 2097184 | tf_op jit(solution)/shard_map/all_to_all | solution.py:22
  75.7 10.3 %shard_map.113 = (f32[512,2048]{1,0:T(8,128)S(1)}, f32[8,512]{1,0:T(8,128)}, bf16[2048,2048]{1,0:T(8,128)(2,1)S(1)}, f32[512,2048]{1,0:T(8,128)S(1)}, bf16[2048,512]{1,0:T(8,128)(2,1)S(1)}) custom-call(bf16[512,2048]{1,0:T(8,128)(2,1)} %bitcast.1.refs_0_, bf16[2048,2048]{1,0:T(8,128)(2,1)} %refs_1_.2, f32[1,2048]{1,0:T(1,128)} %bitcast.69, f32[512,2048]{1,0:T(8,128)} %copy-done.4), custom_call_target="tpu_custom_call" | custom-call | flops 4294967296 | bytes 14688256 | tf_op jit(solution)/shard_map/pallas_call | solution.py:49
  86.7 10.0 %all_to_all.21 = f32[16,3,512]{2,1,0:T(4,128)S(1)} all-to-all(f32[16,3,512]{2,1,0:T(4,128)S(1)} %broadcast_in_dim.5), channel_id=1, replica_groups=mesh['y'=4,'x'=4,'z'=8,'c'=2] {'y','x'}, dimensions={0} | all-to-all | bytes 196608 | tf_op jit(solution)/shard_map/all_to_all | solution.py:22
  97.5 6.9 %shard_map.114 = (bf16[512,2048]{1,0:T(8,128)(2,1)S(1)}, bf16[3,256,1024]{2,1,0:T(8,128)(2,1)S(1)}, bf16[1,256,1024]{2,1,0:T(8,128)(2,1)S(1)}, bf16[1,256,1024]{...) custom-call(s32[11]{0:T(128)S(1)} %stack.44.refs_3_.refs_0_, ...), custom_call_target="tpu_custom_call" | custom-call | flops 4294967296 | bytes 10487808 | tf_op jit(solution)/shard_map/pallas_call | solution.py:49
  104.4 3.4 %collective-permute-done.2 = bf16[3,256,1024]{2,1,0:T(8,128)(2,1)S(1)} collective-permute-done((bf16[3,256,1024]{2,1,0:T(8,128)(2,1)S(1)}, bf16[3,256,1024]{2,1,0:T(8,128)(2,1)S(1)}, u32[]{:S(2)}, u32[]{:S(2)}) %collective-permute-start.2) | collective-permute-done | bytes 1572896 | tf_op jit(solution)/shard_map/ppermute | solution.py:296
  109.3 1.9 %collective-permute-start.3 = (bf16[256,1024]{1,0:T(8,128)(2,1)}, bf16[256,1024]{1,0:T(8,128)(2,1)}, u32[]{:S(2)}, u32[]{:S(2)}) collective-permute-start(bf16[256,1024]{1,0:T(8,128)(2,1)} %get-tuple-element.49), channel_id=1, source_target_pairs={{0,2},{1,15},{2,4},{3,1},{4,6},{5,3},{6,8},{7,5},{8,10},{9,7},{10,... | collective-permute-start | bytes 1572872 | tf_op jit(solution)/shard_map/ppermute | solution.py:303
  111.3 5.8 %shard_map.115 = bf16[512,2048]{1,0:T(8,128)(2,1)} custom-call(bf16[512,2048]{1,0:T(8,128)(2,1)S(1)} %get-tuple-element.27.refs_0_, bf16[2048,2048]{1,0:T(8,128)(2,1)S(1)} %get-tuple-element.28.refs_1_), custom_call_target="tpu_custom_call" | custom-call | flops 4294967296 | bytes 10485760 | tf_op jit(solution)/shard_map/pallas_call | solution.py:49
  117.1 6.6 %all-to-all-start.3 = ((bf16[16,32,2048]{2,1,0:T(8,128)(2,1)}), bf16[16,32,2048]{2,1,0:T(8,128)(2,1)}, u32[]{:S(2)}, u32[]{:S(2)}) async-start(bf16[16,32,2048]{2,1,0:T(8,128)(2,1)} %bitcast.15), calls=%async_computation.3 | async-start | bytes 4194304 | tf_op jit(solution)/shard_map/all_to_all | solution.py:22
  123.7 3.5 %collective-permute-start.8 = (bf16[1,256,1024]{2,1,0:T(8,128)(2,1)}, bf16[1,256,1024]{2,1,0:T(8,128)(2,1)S(1)}, u32[]{:S(2)}, u32[]{:S(2)}) collective-permute-start(bf16[1,256,1024]{2,1,0:T(8,128)(2,1)} %copy-done.7), channel_id=1, source_target_pairs={{0,1},{1,0},{2,3},{3,2},{4,5},{5,4},{6,7},{7,6},{8,9},{9,8},{10,11... | collective-permute-start | bytes 1572872 | tf_op jit(solution)/shard_map/ppermute | solution.py:296
  130.8 1.6 collective-permute-start.7
  132.4 5.4 %collective-permute-done.9 = bf16[256,1024]{1,0:T(8,128)(2,1)S(1)} collective-permute-done((bf16[256,1024]{1,0:T(8,128)(2,1)}, bf16[256,1024]{1,0:T(8,128)(2,1)S(1)}, u32[]{:S(2)}, u32[]{:S(2)}) %collective-permute-start.9) | collective-permute-done | bytes 524320 | tf_op jit(solution)/shard_map/ppermute | solution.py:303
  138.9 4.5 %collective-permute-done.4 = bf16[256,1024]{1,0:T(8,128)(2,1)S(1)} collective-permute-done((bf16[256,1024]{1,0:T(8,128)(2,1)S(1)}, bf16[256,1024]{1,0:T(8,128)(2,1)S(1)}, u32[]{:S(2)}, u32[]{:S(2)}) %collective-permute-start.4) | collective-permute-done | bytes 524320 | tf_op jit(solution)/shard_map/ppermute | solution.py:303
  145.8 3.7 %collective-permute-done.10 = bf16[256,1024]{1,0:T(8,128)(2,1)S(1)} collective-permute-done((bf16[256,1024]{1,0:T(8,128)(2,1)}, bf16[256,1024]{1,0:T(8,128)(2,1)S(1)}, u32[]{:S(2)}, u32[]{:S(2)}) %collective-permute-start.10) | collective-permute-done | bytes 524320 | tf_op jit(solution)/shard_map/ppermute | solution.py:303
  149.5 2.1 %fusion.1 = bf16[256,1024]{1,0:T(8,128)(2,1)} fusion(bf16[256,1024]{1,0:T(8,128)(2,1)S(1)} %collective-permute-done.10, bf16[1,256,1024]{2,1,0:T(8,128)(2,1)} %collective-permute-done.7, bf16[1,256,1024]{2,1,0:T(8,128)(2,1)S(1)} %get-tuple-element.38), kind=kLoop, calls=%fused_computation.7 | loop fusion | flops 1572864 | bytes 2097152 | tf_op jit(solution)/shard_map/convert_element_type | solution.py:331
  151.6 3.5 %collective-permute-done.5 = bf16[256,1024]{1,0:T(8,128)(2,1)S(1)} collective-permute-done((bf16[256,1024]{1,0:T(8,128)(2,1)}, bf16[256,1024]{1,0:T(8,128)(2,1)S(1)}, u32[]{:S(2)}, u32[]{:S(2)}) %collective-permute-start.5) | collective-permute-done | bytes 524320 | tf_op jit(solution)/shard_map/ppermute | solution.py:303
  156.6 2.0 %convert_reduce_fusion = f32[32,2048]{1,0:T(8,128)S(1)} fusion(bf16[16,32,2048]{2,1,0:T(8,128)(2,1)} %all-to-all-done.3), kind=kLoop, calls=%fused_computation | loop fusion | flops 2031616 | bytes 2359296 | tf_op jit(solution)/shard_map/reduce_sum | solution.py:28
  158.8 3.4 %collective-permute-done.11 = bf16[256,1024]{1,0:T(8,128)(2,1)S(1)} collective-permute-done((bf16[256,1024]{1,0:T(8,128)(2,1)}, bf16[256,1024]{1,0:T(8,128)(2,1)S(1)}, u32[]{:S(2)}, u32[]{:S(2)}) %collective-permute-start.11) | collective-permute-done | bytes 524320 | tf_op jit(solution)/shard_map/ppermute | solution.py:303
  163.2 4.7 %collective-permute-done.6 = bf16[256,1024]{1,0:T(8,128)(2,1)S(1)} collective-permute-done((bf16[256,1024]{1,0:T(8,128)(2,1)S(1)}, bf16[256,1024]{1,0:T(8,128)(2,1)S(1)}, u32[]{:S(2)}, u32[]{:S(2)}) %collective-permute-start.6) | collective-permute-done | bytes 524320 | tf_op jit(solution)/shard_map/ppermute | solution.py:303
  168.8 1.7 subtract_multiply_fusion
  (84 shorter events, 21.2 us)
Async XLA Ops:
  4.5 33.1 %copy-start.2 = (bf16[512,2048]{1,0:T(8,128)(2,1)}, bf16[512,2048]{1,0:T(8,128)(2,1)S(1)}, u32[]{:S(2)}) copy-start(bf16[512,2048]{1,0:T(8,128)(2,1)S(1)} %convolution_convert_fusion.refs_2_) | copy-start | bytes 6291460
  41.0 6.8 %copy-start.15 = (s32[512,4]{0,1:T(4,128)S(1)}, s32[512,4]{0,1:T(4,128)}, u32[]{:S(2)}) copy-start(s32[512,4]{0,1:T(4,128)} %param.16) | copy-start | bytes 24580
  41.0 6.9 %copy-start.16 = (f32[512,4]{0,1:T(4,128)S(1)}, f32[512,4]{0,1:T(4,128)}, u32[]{:S(2)}) copy-start(f32[512,4]{0,1:T(4,128)} %param.17) | copy-start | bytes 24580
  41.0 7.3 %copy-start.3 = (bf16[512,2048]{1,0:T(8,128)(2,1)S(1)}, bf16[512,2048]{1,0:T(8,128)(2,1)}, u32[]{:S(2)}) copy-start(bf16[512,2048]{1,0:T(8,128)(2,1)} %copy-done.2) | copy-start | bytes 6291460
  41.0 34.7 %all-to-all-start.1 = ((bf16[16,32,2048]{2,1,0:T(8,128)(2,1)}), bf16[16,32,2048]{2,1,0:T(8,128)(2,1)}, u32[]{:S(2)}, u32[]{:S(2)}) async-start(bf16[16,32,2048]{2,1,0:T(8,128)(2,1)} %broadcast_in_dim.4), calls=%async_computation.1 | async-start | bytes 4194304 | tf_op jit(solution)/shard_map/all_to_all | solution.py:22
  104.4 12.7 %copy-start.5 = (bf16[1,256,1024]{2,1,0:T(8,128)(2,1)}, bf16[1,256,1024]{2,1,0:T(8,128)(2,1)S(1)}, u32[]{:S(2)}) copy-start(bf16[1,256,1024]{2,1,0:T(8,128)(2,1)S(1)} %get-tuple-element.34) | copy-start | bytes 1572868
  104.4 12.7 %copy-start.6 = (bf16[1,256,1024]{2,1,0:T(8,128)(2,1)}, bf16[1,256,1024]{2,1,0:T(8,128)(2,1)S(1)}, u32[]{:S(2)}) copy-start(bf16[1,256,1024]{2,1,0:T(8,128)(2,1)S(1)} %get-tuple-element.33) | copy-start | bytes 1572868
  104.4 12.7 %copy-start.7 = (bf16[1,256,1024]{2,1,0:T(8,128)(2,1)}, bf16[1,256,1024]{2,1,0:T(8,128)(2,1)S(1)}, u32[]{:S(2)}) copy-start(bf16[1,256,1024]{2,1,0:T(8,128)(2,1)S(1)} %get-tuple-element.41) | copy-start | bytes 1572868
  104.4 3.4 %collective-permute-start.2 = (bf16[3,256,1024]{2,1,0:T(8,128)(2,1)S(1)}, bf16[3,256,1024]{2,1,0:T(8,128)(2,1)S(1)}, u32[]{:S(2)}, u32[]{:S(2)}) collective-permute-start(bf16[3,256,1024]{2,1,0:T(8,128)(2,1)S(1)} %get-tuple-element.35), channel_id=1, source_target_pairs={{0,1},{1,0},{2,3},{3,2},{4,5},{5,4},{6,7},{7,6},{8,9},{9,8},{10,11... | collective-permute-start | bytes 4718600 | tf_op jit(solution)/shard_map/ppermute | solution.py:296
  109.3 18.7 %collective-permute-start.3 = (bf16[256,1024]{1,0:T(8,128)(2,1)}, bf16[256,1024]{1,0:T(8,128)(2,1)}, u32[]{:S(2)}, u32[]{:S(2)}) collective-permute-start(bf16[256,1024]{1,0:T(8,128)(2,1)} %get-tuple-element.49), channel_id=1, source_target_pairs={{0,2},{1,15},{2,4},{3,1},{4,6},{5,3},{6,8},{7,5},{8,10},{9,7},{10,... | collective-permute-start | bytes 1572872 | tf_op jit(solution)/shard_map/ppermute | solution.py:303
  117.1 39.5 %all-to-all-start.3 = ((bf16[16,32,2048]{2,1,0:T(8,128)(2,1)}), bf16[16,32,2048]{2,1,0:T(8,128)(2,1)}, u32[]{:S(2)}, u32[]{:S(2)}) async-start(bf16[16,32,2048]{2,1,0:T(8,128)(2,1)} %bitcast.15), calls=%async_computation.3 | async-start | bytes 4194304 | tf_op jit(solution)/shard_map/all_to_all | solution.py:22
  123.7 8.7 %collective-permute-start.8 = (bf16[1,256,1024]{2,1,0:T(8,128)(2,1)}, bf16[1,256,1024]{2,1,0:T(8,128)(2,1)S(1)}, u32[]{:S(2)}, u32[]{:S(2)}) collective-permute-start(bf16[1,256,1024]{2,1,0:T(8,128)(2,1)} %copy-done.7), channel_id=1, source_target_pairs={{0,1},{1,0},{2,3},{3,2},{4,5},{5,4},{6,7},{7,6},{8,9},{9,8},{10,11... | collective-permute-start | bytes 1572872 | tf_op jit(solution)/shard_map/ppermute | solution.py:296
  127.2 10.6 %collective-permute-start.9 = (bf16[256,1024]{1,0:T(8,128)(2,1)}, bf16[256,1024]{1,0:T(8,128)(2,1)S(1)}, u32[]{:S(2)}, u32[]{:S(2)}) collective-permute-start(bf16[256,1024]{1,0:T(8,128)(2,1)} %get-tuple-element.50), channel_id=1, source_target_pairs={{0,2},{1,15},{2,4},{3,1},{4,6},{5,3},{6,8},{7,5},{8,10},{9,7},{10,... | collective-permute-start | bytes 1572872 | tf_op jit(solution)/shard_map/ppermute | solution.py:303
  127.3 11.7 %collective-permute-start.1 = (bf16[1,256,1024]{2,1,0:T(8,128)(2,1)}, bf16[1,256,1024]{2,1,0:T(8,128)(2,1)S(1)}, u32[]{:S(2)}, u32[]{:S(2)}) collective-permute-start(bf16[1,256,1024]{2,1,0:T(8,128)(2,1)} %copy-done.6), channel_id=1, source_target_pairs={{0,1},{1,0},{2,3},{3,2},{4,5},{5,4},{6,7},{7,6},{8,9},{9,8},{10,11... | collective-permute-start | bytes 1572872 | tf_op jit(solution)/shard_map/ppermute | solution.py:296
  129.7 13.8 %collective-permute-start.4 = (bf16[256,1024]{1,0:T(8,128)(2,1)S(1)}, bf16[256,1024]{1,0:T(8,128)(2,1)S(1)}, u32[]{:S(2)}, u32[]{:S(2)}) collective-permute-start(bf16[256,1024]{1,0:T(8,128)(2,1)S(1)} %fusion.2), channel_id=1, source_target_pairs={{0,2},{1,15},{2,4},{3,1},{4,6},{5,3},{6,8},{7,5},{8,10},{9,7},{10,... | collective-permute-start | bytes 1572872 | tf_op jit(solution)/shard_map/ppermute | solution.py:303
  130.8 15.0 %collective-permute-start.7 = (bf16[1,256,1024]{2,1,0:T(8,128)(2,1)}, bf16[1,256,1024]{2,1,0:T(8,128)(2,1)}, u32[]{:S(2)}, u32[]{:S(2)}) collective-permute-start(bf16[1,256,1024]{2,1,0:T(8,128)(2,1)} %get-tuple-element.39), channel_id=1, source_target_pairs={{0,1},{1,0},{2,3},{3,2},{4,5},{5,4},{6,7},{7,6},{8,9},{9,8},{10,11... | collective-permute-start | bytes 1572872 | tf_op jit(solution)/shard_map/ppermute | solution.py:296
  132.4 19.2 %collective-permute-start = (bf16[1,256,1024]{2,1,0:T(8,128)(2,1)}, bf16[1,256,1024]{2,1,0:T(8,128)(2,1)}, u32[]{:S(2)}, u32[]{:S(2)}) collective-permute-start(bf16[1,256,1024]{2,1,0:T(8,128)(2,1)} %get-tuple-element.31), channel_id=1, source_target_pairs={{0,1},{1,0},{2,3},{3,2},{4,5},{5,4},{6,7},{7,6},{8,9},{9,8},{10,11... | collective-permute-start | bytes 1572872 | tf_op jit(solution)/shard_map/ppermute | solution.py:296
  138.9 10.6 %collective-permute-start.10 = (bf16[256,1024]{1,0:T(8,128)(2,1)}, bf16[256,1024]{1,0:T(8,128)(2,1)S(1)}, u32[]{:S(2)}, u32[]{:S(2)}) collective-permute-start(bf16[256,1024]{1,0:T(8,128)(2,1)} %fusion), channel_id=1, source_target_pairs={{0,2},{1,15},{2,4},{3,1},{4,6},{5,3},{6,8},{7,5},{8,10},{9,7},{10,... | collective-permute-start | bytes 1572872 | tf_op jit(solution)/shard_map/ppermute | solution.py:303
  144.5 10.6 %collective-permute-start.5 = (bf16[256,1024]{1,0:T(8,128)(2,1)}, bf16[256,1024]{1,0:T(8,128)(2,1)S(1)}, u32[]{:S(2)}, u32[]{:S(2)}) collective-permute-start(bf16[256,1024]{1,0:T(8,128)(2,1)} %fusion.3), channel_id=1, source_target_pairs={{0,2},{1,15},{2,4},{3,1},{4,6},{5,3},{6,8},{7,5},{8,10},{9,7},{10,... | collective-permute-start | bytes 1572872 | tf_op jit(solution)/shard_map/ppermute | solution.py:303
  151.6 10.6 %collective-permute-start.11 = (bf16[256,1024]{1,0:T(8,128)(2,1)}, bf16[256,1024]{1,0:T(8,128)(2,1)S(1)}, u32[]{:S(2)}, u32[]{:S(2)}) collective-permute-start(bf16[256,1024]{1,0:T(8,128)(2,1)} %fusion.1), channel_id=1, source_target_pairs={{0,2},{1,15},{2,4},{3,1},{4,6},{5,3},{6,8},{7,5},{8,10},{9,7},{10,... | collective-permute-start | bytes 1572872 | tf_op jit(solution)/shard_map/ppermute | solution.py:303
  156.5 12.4 %copy-start.18 = (f32[32]{0:T(128)S(1)}, f32[32]{0:T(128)}, u32[]{:S(2)}) copy-start(f32[32]{0:T(128)} %copy-done.17) | copy-start | bytes 388
  156.5 11.4 %collective-permute-start.6 = (bf16[256,1024]{1,0:T(8,128)(2,1)S(1)}, bf16[256,1024]{1,0:T(8,128)(2,1)S(1)}, u32[]{:S(2)}, u32[]{:S(2)}) collective-permute-start(bf16[256,1024]{1,0:T(8,128)(2,1)S(1)} %fusion.4), channel_id=1, source_target_pairs={{0,2},{1,15},{2,4},{3,1},{4,6},{5,3},{6,8},{7,5},{8,10},{9,7},{10,... | collective-permute-start | bytes 1572872 | tf_op jit(solution)/shard_map/ppermute | solution.py:303
  163.1 7.5 %collective-permute-start.12 = (bf16[128,1024]{1,0:T(8,128)(2,1)S(1)}, bf16[128,1024]{1,0:T(8,128)(2,1)S(1)}, u32[]{:S(2)}, u32[]{:S(2)}) collective-permute-start(bf16[128,1024]{1,0:T(8,128)(2,1)S(1)} %fusion.9), channel_id=1, source_target_pairs={{0,1},{1,0},{2,3},{3,2},{4,5},{5,4},{6,7},{7,6},{8,9},{9,8},{10,11... | collective-permute-start | bytes 786440 | tf_op jit(solution)/shard_map/ppermute | solution.py:296
  168.7 1.8 %collective-permute-start.13 = (bf16[128,1024]{1,0:T(8,128)(2,1)S(1)}, bf16[128,1024]{1,0:T(8,128)(2,1)S(1)}, u32[]{:S(2)}, u32[]{:S(2)}) collective-permute-start(bf16[128,1024]{1,0:T(8,128)(2,1)S(1)} %fusion.7), channel_id=1, source_target_pairs={{0,1},{1,0},{2,3},{3,2},{4,5},{5,4},{6,7},{7,6},{8,9},{9,8},{10,11... | collective-permute-start | bytes 786440 | tf_op jit(solution)/shard_map/ppermute | solution.py:296
  (11 other events, 16.4 us)

commit v2 on v1

--- a/solution.py
+++ b/solution.py
@@ -103,7 +103,7 @@
     columns = vocab.shape[1]
     blocks = [slice(at, at + SCORE_BLOCK) for at in range(0, columns, SCORE_BLOCK)]
 
-    def kernel(rows_ref, vocab_hbm, bias_ref, wanted_hbm, out_ref, stats_ref, vocab_ref, wanted_ref, turned_ref, sems):
+    def kernel(rows_ref, vocab_hbm, bias_ref, wanted_hbm, out_ref, stats_ref, wanted_ref, turned_ref, vocab_ref, sems):
         deep = width // 4
         load_vocab = [
             pltpu.make_async_copy(
@@ -159,34 +159,41 @@
         packed = jnp.where(lane == 0, row_top, jnp.where(lane == 1, row_total, row_target))
         stats_ref[...] = packed.T[:8]
 
-    scores, stats, near_vocab, near_wanted, turned = call(
+    scores, stats, near_wanted, turned = call(
         kernel,
         (1,),
         [NEAR, HBM, pl.BlockSpec((1, columns), lambda i: (0, 0)), HBM],
-        [NEAR, pl.BlockSpec((8, tokens), lambda i: (0, 0)), NEAR, NEAR, NEAR],
+        [NEAR, pl.BlockSpec((8, tokens), lambda i: (0, 0)), NEAR, NEAR],
         [
             pltpu.VMEM((tokens, columns), F32),
             jax.ShapeDtypeStruct((8, tokens), F32),
-            pltpu.VMEM(vocab.shape, vocab.dtype),
             pltpu.VMEM(wanted.shape, wanted.dtype),
             pltpu.VMEM((width, tokens), rows.dtype),
         ],
         [rows, vocab, bias.reshape(1, columns), wanted],
         2 * tokens * width * columns,
-        scratch=[pltpu.SemaphoreType.DMA((5,))],
-        vmem=42,
-    )
-    return scores, stats[:3], near_vocab, near_wanted, turned
+        scratch=[pltpu.VMEM(vocab.shape, vocab.dtype), pltpu.SemaphoreType.DMA((5,))],
+        vmem=50,
+    )
+    return scores, stats[:3], near_wanted, turned
+
+
+def multiply_blocks(index_ref, rows_ref, kept_ref, outs, lists, chunk):
+    for out, some in zip(outs, lists):
+        for k, (place, slot) in enumerate(some):
+            side = index_ref[0] if slot == 0 else 1 - index_ref[0]
+            start = pl.multiple_of(index_ref[place] * chunk, chunk)
+            out[k] = jnp.dot(
+                rows_ref[pl.ds(start, chunk)], kept_ref[side], preferred_element_type=F32
+            ).astype(BF16)
 
 
 def gradients(scores, log_norm, wanted, rows, index, lists, chunk):
     tokens, columns = scores.shape
-    width = rows.shape[0]
     half = columns // 2
     part = 128
 
-    def kernel(index_ref, scores_ref, norm_ref, wanted_ref, rows_ref, grads_ref, *refs):
-        outs, kept = refs[:-1], refs[-1]
+    def kernel(index_ref, scores_ref, norm_ref, wanted_ref, rows_ref, grads_ref, kept_ref, *outs):
         norms = jnp.broadcast_to(norm_ref[...], (LANES, tokens)).T
         for i in range(0, tokens, part):
             norm = norms[i : i + part]
@@ -196,28 +203,40 @@
                 probability = jnp.exp(scores_ref[cell] - norm)
                 value = (loss_scale * (probability * factor - wanted_ref[cell])).astype(BF16)
                 grads_ref[cell] = value
-                kept[at // half, cell[0], at % half : at % half + LANES] = value
-        for out, some in zip(outs, lists):
-            for k, (place, slot) in enumerate(some):
-                side = index_ref[0] if slot == 0 else 1 - index_ref[0]
-                start = pl.multiple_of(index_ref[place] * chunk, chunk)
-                out[k] = jnp.dot(
-                    rows_ref[pl.ds(start, chunk)], kept[side], preferred_element_type=F32
-                ).astype(BF16)
+                kept_ref[at // half, cell[0], at % half : at % half + LANES] = value
+        multiply_blocks(index_ref, rows_ref, kept_ref, outs, lists, chunk)
 
     results = call(
         kernel,
         (1,),
         [NEAR, pl.BlockSpec((1, tokens), lambda i, idx: (0, 0)), NEAR, NEAR],
-        [NEAR] * (1 + len(lists)),
-        [pltpu.VMEM(scores.shape, BF16)]
+        [NEAR] * (2 + len(lists)),
+        [pltpu.VMEM(scores.shape, BF16), pltpu.VMEM((2, tokens, half), BF16)]
         + [pltpu.VMEM((len(some), chunk, half), BF16) for some in lists],
         [scores, log_norm[None], wanted, rows],
-        2 * width * columns * tokens,
-        scratch=[pltpu.VMEM((2, tokens, half), BF16)],
+        2 * chunk * half * tokens * sum(len(some) for some in lists),
         scalars=index,
     )
-    return results[0], results[1:]
+    return results[0], results[1], results[2:]
+
+
+def block_products(rows, kept, index, lists, chunk):
+    tokens = rows.shape[1]
+    half = kept.shape[2]
+
+    def kernel(index_ref, rows_ref, kept_ref, *outs):
+        multiply_blocks(index_ref, rows_ref, kept_ref, outs, lists, chunk)
+
+    return call(
+        kernel,
+        (1,),
+        [NEAR, NEAR],
+        [NEAR] * len(lists),
+        [pltpu.VMEM((len(some), chunk, half), BF16) for some in lists],
+        [rows, kept],
+        2 * chunk * half * tokens * sum(len(some) for some in lists),
+        scalars=index,
+    )
 
 
 def row_gradients(grads, vocab):
@@ -280,7 +299,7 @@
     )
 
     wanted = wanted_matrix(ids, target_weights, columns, (branch_parts, index))
-    scores, stats, near_vocab, near_wanted, normed_rows = scored(
+    scores, stats, near_wanted, normed_rows = scored(
         gathered, vocab, vocab_bias, wanted
     )
     n_vp = lax.axis_size(VP)
@@ -311,21 +330,26 @@
     first = [(far, 0), (far - 1, 1), (far - 1, 0)]
     rest = [(d, lane) for d in range(far - 2, 0, -1) for lane in (1, 0)]
     owned = first + rest + [(0, 0), (0, 1)]
-    grads, products = gradients(
+    grads, kept, (theirs_first,) = gradients(
         scores,
         log_norm,
         near_wanted,
         normed_rows,
         index,
-        [[their_block(*key) for key in first]]
-        + [[their_block(*key)] for key in rest]
-        + [[own_block(*key)] for key in owned],
+        [[their_block(*key) for key in first]],
         chunk,
     )
-    passed_first = swapped(products[0])
+    passed_first = swapped(theirs_first)
+    products = block_products(
+        normed_rows,
+        kept,
+        index,
+        [[own_block(*key)] for key in owned] + [[their_block(*key)] for key in rest],
+        chunk,
+    )
     passed = {key: passed_first[at] for at, key in enumerate(first)}
-    passed.update({key: swapped(block)[0] for key, block in zip(rest, products[1:])})
-    own = {key: block[0] for key, block in zip(owned, products[1 + len(rest) :])}
+    passed.update({key: swapped(block)[0] for key, block in zip(rest, products[len(owned) :])})
+    own = {key: block[0] for key, block in zip(owned, products)}
 
     def message(key, *carried):
         return sum(x.astype(F32) for x in (own[key], passed[key], *carried)).astype(BF16)
@@ -351,7 +375,7 @@
         [jnp.where(core == 0, lanes[0], lanes[1]), jnp.where(core == 0, lanes[1], lanes[0])], axis=1
     )
 
-    row_parts = row_gradients(grads, near_vocab)
+    row_parts = row_gradients(grads, vocab)
     row_grad = summed_over(row_parts, VP)
     upstream = row_grad * final_gain
     stream_grad = inverse * (

time: 175 us -> 174 us (level)
  waiting for transfers between devices: 51 us -> 47.6 us
    ppermute x7, waiting for transfers between devices: 3.42 us -> 0.02 us  [swapped(): return lax.ppermute(x, 'c', [(0, 1), (1, 0)])]
    pallas_call x4 -> x5, Pallas kernels: 26.1 us -> 27.5 us  [call(): pl.pallas_call(body, grid_spec=pltpu.PrefetchScalarGridSpec(num_scalar_pr...]
    unnamed x40 -> x44, local copies, waits for them, and re-layouts: 6.3 us -> 6.27 us
  transfers between devices with their start and end apart: 16 -> 16, of which waited for: 8 -> 7; matrix products, arithmetic and copies ran while one was open for 7% -> 8% of each run, Pallas kernels for 5% -> 8%
where the time goes in v2:
time: 174 us; the launch traced here: 172 us
  waiting for transfers between devices  47.6 us (27%)
  blocking collectives  43.1 us (25%)
  Pallas kernels  27.5 us (16%)
  starting transfers between devices  23.2 us (13%)
  other arithmetic  17 us (10%)
  local copies, waits for them, and re-layouts  9.99 us (6%)
  matrix products  2.3 us (1%)
    all_to_all x2, blocking collectives, exchange(): return lax.all_to_all(parts, axis, split_axis=0, concat_axis=0, tiled=True)  43.1 us
    pallas_call x5, Pallas kernels, call(): pl.pallas_call(body, grid_spec=pltpu.PrefetchScalarGridSpec(num_scalar_pr...  27.5 us
    ppermute x7, waiting for transfers between devices, sent(): return lax.ppermute(x.astype(BF16), DP, ring)  25.2 us
    all_to_all x2, waiting for transfers between devices, exchange(): return lax.all_to_all(parts, axis, split_axis=0, concat_axis=0, tiled=True)  22.4 us
    all_to_all x2, starting transfers between devices, exchange(): return lax.all_to_all(parts, axis, split_axis=0, concat_axis=0, tiled=True)  13.4 us
    convert_element_type x6, other arithmetic, message(): sum((x.astype(F32) for x in (own[key], passed[key], *carried))).astype(BF16)  8.92 us
    ppermute x7, starting transfers between devices, swapped(): return lax.ppermute(x, 'c', [(0, 1), (1, 0)])  6.75 us
    unnamed x44, local copies, waits for them, and re-layouts  6.27 us
  transfers between devices with their start and end apart: 16, of which 7 were waited for; matrix products, arithmetic and copies ran while one was open for 8% of the time, Pallas kernels for 8%

profile of v2, /device:TPU:24, one launch (start us, length us, event | category | flops | bytes accessed | tf_op | source)
XLA Modules:
  0.0 171.7 jit_solution(16333996664839006473)
XLA Ops:
  2.2 2.3 %convolution_convert_fusion.refs_2_ = bf16[512,2048]{1,0:T(8,128)(2,1)S(1)} fusion(bf16[512,512]{1,0:T(8,128)(2,1)} %param.9, bf16[512,2048]{1,0:T(8,128)(2,1)S(1)} %copy-done), kind=kOutput, calls=%fused_computation.2 | convolution fusion | flops 1074790400 | bytes 4718592 | tf_op jit(solution)/shard_map/dot_general | solution.py:284
  4.5 33.1 %all_to_all.20 = bf16[16,32,2048]{2,1,0:T(8,128)(2,1)S(1)} all-to-all(bf16[16,32,2048]{2,1,0:T(8,128)(2,1)S(1)} %bitcast.67), channel_id=1, replica_groups=mesh['y'=4,'x'=4,'z'=8,'c'=2] {'y','x'}, dimensions={0} | all-to-all | bytes 4194304 | tf_op jit(solution)/shard_map/all_to_all | solution.py:22
  40.9 6.8 %all-to-all-start.1 = ((bf16[16,32,2048]{2,1,0:T(8,128)(2,1)}), bf16[16,32,2048]{2,1,0:T(8,128)(2,1)}, u32[]{:S(2)}, u32[]{:S(2)}) async-start(bf16[16,32,2048]{2,1,0:T(8,128)(2,1)} %broadcast_in_dim.4), calls=%async_computation.1 | async-start | bytes 4194304 | tf_op jit(solution)/shard_map/all_to_all | solution.py:22
  48.2 3.1 %shard_map.112.refs_3_ = f32[512,2048]{1,0:T(8,128)S(1)} custom-call(s32[512,4]{1,0:T(8,128)S(1)} %broadcast_subtract_fusion.refs_0_, f32[512,4]{1,0:T(8,128)S(1)} %copy.23.refs_1_, bf16[512,2048]{1,0:T(8,128)(2,1)S(1)} %copy-done.3, s32[11]{0:T(128)S(1)} %stack.44.refs_3_.refs_0_), custom_call_target="tpu_custom_call" | custom-call | flops 8388608 | bytes 16384 | tf_op jit(solution)/shard_map/pallas_call | solution.py:49
  51.3 1.9 %copy-done.4 = f32[512,2048]{1,0:T(8,128)} copy-done((f32[512,2048]{1,0:T(8,128)}, f32[512,2048]{1,0:T(8,128)S(1)}, u32[]{:S(2)}) %copy-start.4) | copy-done | bytes 4194328
  53.3 22.4 %all-to-all-done.1 = bf16[16,32,2048]{2,1,0:T(8,128)(2,1)} async-done(((bf16[16,32,2048]{2,1,0:T(8,128)(2,1)}), bf16[16,32,2048]{2,1,0:T(8,128)(2,1)}, u32[]{:S(2)}, u32[]{:S(2)}) %all-to-all-start.1) | async-done | bytes 2097184 | tf_op jit(solution)/shard_map/all_to_all | solution.py:22
  75.6 10.3 %shard_map.113 = (f32[512,2048]{1,0:T(8,128)S(1)}, f32[8,512]{1,0:T(8,128)}, f32[512,2048]{1,0:T(8,128)S(1)}, bf16[2048,512]{1,0:T(8,128)(2,1)S(1)}) custom-call(bf16[512,2048]{1,0:T(8,128)(2,1)} %bitcast.1.refs_0_, bf16[2048,2048]{1,0:T(8,128)(2,1)} %refs_1_.4, f32[1,2048]{1,0:T(1,128)} %bitcast.71, f32[512,2048]{1,0:T(8,128)} %copy-done.4), custom_call_target="tpu_custom_call" | custom-call | flops 4294967296 | bytes 14688256 | tf_op jit(solution)/shard_map/pallas_call | solution.py:49
  86.7 10.0 %all_to_all.21 = f32[16,3,512]{2,1,0:T(4,128)S(1)} all-to-all(f32[16,3,512]{2,1,0:T(4,128)S(1)} %broadcast_in_dim.5), channel_id=1, replica_groups=mesh['y'=4,'x'=4,'z'=8,'c'=2] {'y','x'}, dimensions={0} | all-to-all | bytes 196608 | tf_op jit(solution)/shard_map/all_to_all | solution.py:22
  97.4 3.1 %shard_map.114 = (bf16[512,2048]{1,0:T(8,128)(2,1)S(1)}, bf16[2,512,1024]{2,1,0:T(8,128)(2,1)S(1)}, bf16[3,256,1024]{2,1,0:T(8,128)(2,1)S(1)}) custom-call(s32[11]{0:T(128)S(1)} %stack.44.refs_3_.refs_0_, f32[512,2048]{1,0:T(8,128)S(1)} %get-tuple-element.24.refs_1_, f32[1,512]{1,0:T(1,128)S(1)} %bitcast.68, f32[512,2048]{1,0:T(8,128)S(1)} %get-tuple-element.25.refs_3_, ...), custom_call_target="tpu_custom_call" | custom-call | flops 805306368 | bytes 10487808 | tf_op jit(solution)/shard_map/pallas_call | solution.py:49
  100.8 5.2 %shard_map.116 = (bf16[1,256,1024]{2,1,0:T(8,128)(2,1)S(1)}, bf16[1,256,1024]{2,1,0:T(8,128)(2,1)S(1)}, bf16[1,256,1024]{2,1,0:T(8,128)(2,1)S(1)}, bf16[1,256,10...) custom-call(s32[11]{0:T(128)S(1)} %stack.44.refs_3_.refs_0_, ...), custom_call_target="tpu_custom_call" | custom-call | flops 3489660928 | bytes 4194304 | tf_op jit(solution)/shard_map/pallas_call | solution.py:49
  106.1 1.7 %fusion.5 = (bf16[256,1024]{1,0:T(8,128)(2,1)}, bf16[256,1024]{1,0:T(8,128)(2,1)}) fusion(bf16[1,256,1024]{2,1,0:T(8,128)(2,1)S(1)} %get-tuple-element.36, bf16[3,256,1024]{2,1,0:T(8,128)(2,1)S(1)} %collective-permute-done.2, bf16[1,256,1024]{2,1,0:T(8,128)(2,1)S(1)} %get-tuple-element.42), kind=kLoop, calls=%fused_computation.16 | loop fusion | flops 2097152 | bytes 3145728 | tf_op jit(solution)/shard_map/convert_element_type | solution.py:355
  107.8 1.9 %collective-permute-start.3 = (bf16[256,1024]{1,0:T(8,128)(2,1)}, bf16[256,1024]{1,0:T(8,128)(2,1)}, u32[]{:S(2)}, u32[]{:S(2)}) collective-permute-start(bf16[256,1024]{1,0:T(8,128)(2,1)} %get-tuple-element.49), channel_id=1, source_target_pairs={{0,2},{1,15},{2,4},{3,1},{4,6},{5,3},{6,8},{7,5},{8,10},{9,7},{10,... | collective-permute-start | bytes 1572872 | tf_op jit(solution)/shard_map/ppermute | solution.py:322
  109.7 5.8 %shard_map.115 = bf16[512,2048]{1,0:T(8,128)(2,1)} custom-call(bf16[512,2048]{1,0:T(8,128)(2,1)S(1)} %get-tuple-element.27.refs_0_, bf16[2048,2048]{1,0:T(8,128)(2,1)S(1)} %bitcast.70), custom_call_target="tpu_custom_call" | custom-call | flops 4294967296 | bytes 10485760 | tf_op jit(solution)/shard_map/pallas_call | solution.py:49
  115.6 6.6 %all-to-all-start.3 = ((bf16[16,32,2048]{2,1,0:T(8,128)(2,1)}), bf16[16,32,2048]{2,1,0:T(8,128)(2,1)}, u32[]{:S(2)}, u32[]{:S(2)}) async-start(bf16[16,32,2048]{2,1,0:T(8,128)(2,1)} %bitcast.15), calls=%async_computation.3 | async-start | bytes 4194304 | tf_op jit(solution)/shard_map/all_to_all | solution.py:22
  122.2 3.8 %collective-permute-start.8 = (bf16[1,256,1024]{2,1,0:T(8,128)(2,1)}, bf16[1,256,1024]{2,1,0:T(8,128)(2,1)S(1)}, u32[]{:S(2)}, u32[]{:S(2)}) collective-permute-start(bf16[1,256,1024]{2,1,0:T(8,128)(2,1)} %copy-done.7), channel_id=1, source_target_pairs={{0,1},{1,0},{2,3},{3,2},{4,5},{5,4},{6,7},{7,6},{8,9},{9,8},{10,11... | collective-permute-start | bytes 1572872 | tf_op jit(solution)/shard_map/ppermute | solution.py:315
  131.2 5.4 %collective-permute-done.9 = bf16[256,1024]{1,0:T(8,128)(2,1)S(1)} collective-permute-done((bf16[256,1024]{1,0:T(8,128)(2,1)}, bf16[256,1024]{1,0:T(8,128)(2,1)S(1)}, u32[]{:S(2)}, u32[]{:S(2)}) %collective-permute-start.9) | collective-permute-done | bytes 524320 | tf_op jit(solution)/shard_map/ppermute | solution.py:322
  137.7 4.5 %collective-permute-done.4 = bf16[256,1024]{1,0:T(8,128)(2,1)S(1)} collective-permute-done((bf16[256,1024]{1,0:T(8,128)(2,1)S(1)}, bf16[256,1024]{1,0:T(8,128)(2,1)S(1)}, u32[]{:S(2)}, u32[]{:S(2)}) %collective-permute-start.4) | collective-permute-done | bytes 524320 | tf_op jit(solution)/shard_map/ppermute | solution.py:322
  144.6 3.7 %collective-permute-done.10 = bf16[256,1024]{1,0:T(8,128)(2,1)S(1)} collective-permute-done((bf16[256,1024]{1,0:T(8,128)(2,1)}, bf16[256,1024]{1,0:T(8,128)(2,1)S(1)}, u32[]{:S(2)}, u32[]{:S(2)}) %collective-permute-start.10) | collective-permute-done | bytes 524320 | tf_op jit(solution)/shard_map/ppermute | solution.py:322
  148.3 2.1 %fusion.1 = bf16[256,1024]{1,0:T(8,128)(2,1)} fusion(bf16[256,1024]{1,0:T(8,128)(2,1)S(1)} %collective-permute-done.10, bf16[1,256,1024]{2,1,0:T(8,128)(2,1)} %collective-permute-done.7, bf16[1,256,1024]{2,1,0:T(8,128)(2,1)S(1)} %get-tuple-element.38), kind=kLoop, calls=%fused_computation.7 | loop fusion | flops 1572864 | bytes 2097152 | tf_op jit(solution)/shard_map/convert_element_type | solution.py:355
  150.4 3.5 %collective-permute-done.5 = bf16[256,1024]{1,0:T(8,128)(2,1)S(1)} collective-permute-done((bf16[256,1024]{1,0:T(8,128)(2,1)}, bf16[256,1024]{1,0:T(8,128)(2,1)S(1)}, u32[]{:S(2)}, u32[]{:S(2)}) %collective-permute-start.5) | collective-permute-done | bytes 524320 | tf_op jit(solution)/shard_map/ppermute | solution.py:322
  155.4 2.0 %convert_reduce_fusion = f32[32,2048]{1,0:T(8,128)S(1)} fusion(bf16[16,32,2048]{2,1,0:T(8,128)(2,1)} %all-to-all-done.3), kind=kLoop, calls=%fused_computation | loop fusion | flops 2031616 | bytes 2359296 | tf_op jit(solution)/shard_map/reduce_sum | solution.py:28
  157.6 3.4 %collective-permute-done.11 = bf16[256,1024]{1,0:T(8,128)(2,1)S(1)} collective-permute-done((bf16[256,1024]{1,0:T(8,128)(2,1)}, bf16[256,1024]{1,0:T(8,128)(2,1)S(1)}, u32[]{:S(2)}, u32[]{:S(2)}) %collective-permute-start.11) | collective-permute-done | bytes 524320 | tf_op jit(solution)/shard_map/ppermute | solution.py:322
  162.0 4.7 %collective-permute-done.6 = bf16[256,1024]{1,0:T(8,128)(2,1)S(1)} collective-permute-done((bf16[256,1024]{1,0:T(8,128)(2,1)S(1)}, bf16[256,1024]{1,0:T(8,128)(2,1)S(1)}, u32[]{:S(2)}, u32[]{:S(2)}) %collective-permute-start.6) | collective-permute-done | bytes 524320 | tf_op jit(solution)/shard_map/ppermute | solution.py:322
  167.7 1.7 subtract_multiply_fusion
  (90 shorter events, 21.6 us)
Async XLA Ops:
  4.5 33.1 %copy-start.2 = (bf16[512,2048]{1,0:T(8,128)(2,1)}, bf16[512,2048]{1,0:T(8,128)(2,1)S(1)}, u32[]{:S(2)}) copy-start(bf16[512,2048]{1,0:T(8,128)(2,1)S(1)} %convolution_convert_fusion.refs_2_) | copy-start | bytes 6291460
  40.9 34.7 %all-to-all-start.1 = ((bf16[16,32,2048]{2,1,0:T(8,128)(2,1)}), bf16[16,32,2048]{2,1,0:T(8,128)(2,1)}, u32[]{:S(2)}, u32[]{:S(2)}) async-start(bf16[16,32,2048]{2,1,0:T(8,128)(2,1)} %broadcast_in_dim.4), calls=%async_computation.1 | async-start | bytes 4194304 | tf_op jit(solution)/shard_map/all_to_all | solution.py:22
  100.5 5.5 %collective-permute-start.2 = (bf16[3,256,1024]{2,1,0:T(8,128)(2,1)S(1)}, bf16[3,256,1024]{2,1,0:T(8,128)(2,1)S(1)}, u32[]{:S(2)}, u32[]{:S(2)}) collective-permute-start(bf16[3,256,1024]{2,1,0:T(8,128)(2,1)S(1)} %get-tuple-element.35), channel_id=1, source_target_pairs={{0,1},{1,0},{2,3},{3,2},{4,5},{5,4},{6,7},{7,6},{8,9},{9,8},{10,11... | collective-permute-start | bytes 4718600 | tf_op jit(solution)/shard_map/ppermute | solution.py:315
  100.8 8.9 %slice-start = ((s8[8388608]{0:T(1024)(128)(4,1)}), s8[4194304]{0:T(1024)(128)(4,1)S(1)}, s32[]{:S(2)}) async-start(s8[8388608]{0:T(1024)(128)(4,1)} %bitcast.69), calls=%async_computation.4 | async-start | bytes 8388608
  100.8 8.9 %slice-start.1 = ((s8[8388608]{0:T(1024)(128)(4,1)}), s8[4194304]{0:T(1024)(128)(4,1)S(1)}, s32[]{:S(2)}) async-start(s8[8388608]{0:T(1024)(128)(4,1)} %bitcast.69), calls=%async_computation.5 | async-start | bytes 8388608
  106.0 9.5 %copy-start.5 = (bf16[1,256,1024]{2,1,0:T(8,128)(2,1)}, bf16[1,256,1024]{2,1,0:T(8,128)(2,1)S(1)}, u32[]{:S(2)}) copy-start(bf16[1,256,1024]{2,1,0:T(8,128)(2,1)S(1)} %get-tuple-element.34) | copy-start | bytes 1572868
  106.0 9.5 %copy-start.6 = (bf16[1,256,1024]{2,1,0:T(8,128)(2,1)}, bf16[1,256,1024]{2,1,0:T(8,128)(2,1)S(1)}, u32[]{:S(2)}) copy-start(bf16[1,256,1024]{2,1,0:T(8,128)(2,1)S(1)} %get-tuple-element.33) | copy-start | bytes 1572868
  106.0 9.5 %copy-start.7 = (bf16[1,256,1024]{2,1,0:T(8,128)(2,1)}, bf16[1,256,1024]{2,1,0:T(8,128)(2,1)S(1)}, u32[]{:S(2)}) copy-start(bf16[1,256,1024]{2,1,0:T(8,128)(2,1)S(1)} %get-tuple-element.41) | copy-start | bytes 1572868
  106.1 9.5 %copy-start.9 = (bf16[3,256,1024]{2,1,0:T(8,128)(2,1)}, bf16[3,256,1024]{2,1,0:T(8,128)(2,1)S(1)}, u32[]{:S(2)}) copy-start(bf16[3,256,1024]{2,1,0:T(8,128)(2,1)S(1)} %collective-permute-done.2) | copy-start | bytes 4718596
  107.8 19.1 %collective-permute-start.3 = (bf16[256,1024]{1,0:T(8,128)(2,1)}, bf16[256,1024]{1,0:T(8,128)(2,1)}, u32[]{:S(2)}, u32[]{:S(2)}) collective-permute-start(bf16[256,1024]{1,0:T(8,128)(2,1)} %get-tuple-element.49), channel_id=1, source_target_pairs={{0,2},{1,15},{2,4},{3,1},{4,6},{5,3},{6,8},{7,5},{8,10},{9,7},{10,... | collective-permute-start | bytes 1572872 | tf_op jit(solution)/shard_map/ppermute | solution.py:322
  115.6 39.8 %all-to-all-start.3 = ((bf16[16,32,2048]{2,1,0:T(8,128)(2,1)}), bf16[16,32,2048]{2,1,0:T(8,128)(2,1)}, u32[]{:S(2)}, u32[]{:S(2)}) async-start(bf16[16,32,2048]{2,1,0:T(8,128)(2,1)} %bitcast.15), calls=%async_computation.3 | async-start | bytes 4194304 | tf_op jit(solution)/shard_map/all_to_all | solution.py:22
  122.2 9.0 %collective-permute-start.8 = (bf16[1,256,1024]{2,1,0:T(8,128)(2,1)}, bf16[1,256,1024]{2,1,0:T(8,128)(2,1)S(1)}, u32[]{:S(2)}, u32[]{:S(2)}) collective-permute-start(bf16[1,256,1024]{2,1,0:T(8,128)(2,1)} %copy-done.7), channel_id=1, source_target_pairs={{0,1},{1,0},{2,3},{3,2},{4,5},{5,4},{6,7},{7,6},{8,9},{9,8},{10,11... | collective-permute-start | bytes 1572872 | tf_op jit(solution)/shard_map/ppermute | solution.py:315
  126.0 10.6 %collective-permute-start.9 = (bf16[256,1024]{1,0:T(8,128)(2,1)}, bf16[256,1024]{1,0:T(8,128)(2,1)S(1)}, u32[]{:S(2)}, u32[]{:S(2)}) collective-permute-start(bf16[256,1024]{1,0:T(8,128)(2,1)} %get-tuple-element.50), channel_id=1, source_target_pairs={{0,2},{1,15},{2,4},{3,1},{4,6},{5,3},{6,8},{7,5},{8,10},{9,7},{10,... | collective-permute-start | bytes 1572872 | tf_op jit(solution)/shard_map/ppermute | solution.py:322
  126.0 11.7 %collective-permute-start.1 = (bf16[1,256,1024]{2,1,0:T(8,128)(2,1)}, bf16[1,256,1024]{2,1,0:T(8,128)(2,1)S(1)}, u32[]{:S(2)}, u32[]{:S(2)}) collective-permute-start(bf16[1,256,1024]{2,1,0:T(8,128)(2,1)} %copy-done.6), channel_id=1, source_target_pairs={{0,1},{1,0},{2,3},{3,2},{4,5},{5,4},{6,7},{7,6},{8,9},{9,8},{10,11... | collective-permute-start | bytes 1572872 | tf_op jit(solution)/shard_map/ppermute | solution.py:315
  128.5 13.8 %collective-permute-start.4 = (bf16[256,1024]{1,0:T(8,128)(2,1)S(1)}, bf16[256,1024]{1,0:T(8,128)(2,1)S(1)}, u32[]{:S(2)}, u32[]{:S(2)}) collective-permute-start(bf16[256,1024]{1,0:T(8,128)(2,1)S(1)} %fusion.2), channel_id=1, source_target_pairs={{0,2},{1,15},{2,4},{3,1},{4,6},{5,3},{6,8},{7,5},{8,10},{9,7},{10,... | collective-permute-start | bytes 1572872 | tf_op jit(solution)/shard_map/ppermute | solution.py:322
  129.6 20.9 %collective-permute-start = (bf16[1,256,1024]{2,1,0:T(8,128)(2,1)}, bf16[1,256,1024]{2,1,0:T(8,128)(2,1)}, u32[]{:S(2)}, u32[]{:S(2)}) collective-permute-start(bf16[1,256,1024]{2,1,0:T(8,128)(2,1)} %get-tuple-element.31), channel_id=1, source_target_pairs={{0,1},{1,0},{2,3},{3,2},{4,5},{5,4},{6,7},{7,6},{8,9},{9,8},{10,11... | collective-permute-start | bytes 1572872 | tf_op jit(solution)/shard_map/ppermute | solution.py:315
  131.2 13.4 %collective-permute-start.7 = (bf16[1,256,1024]{2,1,0:T(8,128)(2,1)}, bf16[1,256,1024]{2,1,0:T(8,128)(2,1)}, u32[]{:S(2)}, u32[]{:S(2)}) collective-permute-start(bf16[1,256,1024]{2,1,0:T(8,128)(2,1)} %get-tuple-element.39), channel_id=1, source_target_pairs={{0,1},{1,0},{2,3},{3,2},{4,5},{5,4},{6,7},{7,6},{8,9},{9,8},{10,11... | collective-permute-start | bytes 1572872 | tf_op jit(solution)/shard_map/ppermute | solution.py:315
  137.7 10.6 %collective-permute-start.10 = (bf16[256,1024]{1,0:T(8,128)(2,1)}, bf16[256,1024]{1,0:T(8,128)(2,1)S(1)}, u32[]{:S(2)}, u32[]{:S(2)}) collective-permute-start(bf16[256,1024]{1,0:T(8,128)(2,1)} %fusion), channel_id=1, source_target_pairs={{0,2},{1,15},{2,4},{3,1},{4,6},{5,3},{6,8},{7,5},{8,10},{9,7},{10,... | collective-permute-start | bytes 1572872 | tf_op jit(solution)/shard_map/ppermute | solution.py:322
  143.3 10.6 %collective-permute-start.5 = (bf16[256,1024]{1,0:T(8,128)(2,1)}, bf16[256,1024]{1,0:T(8,128)(2,1)S(1)}, u32[]{:S(2)}, u32[]{:S(2)}) collective-permute-start(bf16[256,1024]{1,0:T(8,128)(2,1)} %fusion.3), channel_id=1, source_target_pairs={{0,2},{1,15},{2,4},{3,1},{4,6},{5,3},{6,8},{7,5},{8,10},{9,7},{10,... | collective-permute-start | bytes 1572872 | tf_op jit(solution)/shard_map/ppermute | solution.py:322
  150.4 10.6 %collective-permute-start.11 = (bf16[256,1024]{1,0:T(8,128)(2,1)}, bf16[256,1024]{1,0:T(8,128)(2,1)S(1)}, u32[]{:S(2)}, u32[]{:S(2)}) collective-permute-start(bf16[256,1024]{1,0:T(8,128)(2,1)} %fusion.1), channel_id=1, source_target_pairs={{0,2},{1,15},{2,4},{3,1},{4,6},{5,3},{6,8},{7,5},{8,10},{9,7},{10,... | collective-permute-start | bytes 1572872 | tf_op jit(solution)/shard_map/ppermute | solution.py:322
  155.3 12.4 %copy-start.18 = (f32[32]{0:T(128)S(1)}, f32[32]{0:T(128)}, u32[]{:S(2)}) copy-start(f32[32]{0:T(128)} %copy-done.17) | copy-start | bytes 388
  155.3 11.4 %collective-permute-start.6 = (bf16[256,1024]{1,0:T(8,128)(2,1)S(1)}, bf16[256,1024]{1,0:T(8,128)(2,1)S(1)}, u32[]{:S(2)}, u32[]{:S(2)}) collective-permute-start(bf16[256,1024]{1,0:T(8,128)(2,1)S(1)} %fusion.4), channel_id=1, source_target_pairs={{0,2},{1,15},{2,4},{3,1},{4,6},{5,3},{6,8},{7,5},{8,10},{9,7},{10,... | collective-permute-start | bytes 1572872 | tf_op jit(solution)/shard_map/ppermute | solution.py:322
  161.9 7.5 %collective-permute-start.12 = (bf16[128,1024]{1,0:T(8,128)(2,1)S(1)}, bf16[128,1024]{1,0:T(8,128)(2,1)S(1)}, u32[]{:S(2)}, u32[]{:S(2)}) collective-permute-start(bf16[128,1024]{1,0:T(8,128)(2,1)S(1)} %fusion.9), channel_id=1, source_target_pairs={{0,1},{1,0},{2,3},{3,2},{4,5},{5,4},{6,7},{7,6},{8,9},{9,8},{10,11... | collective-permute-start | bytes 786440 | tf_op jit(solution)/shard_map/ppermute | solution.py:315
  167.5 1.8 %collective-permute-start.13 = (bf16[128,1024]{1,0:T(8,128)(2,1)S(1)}, bf16[128,1024]{1,0:T(8,128)(2,1)S(1)}, u32[]{:S(2)}, u32[]{:S(2)}) collective-permute-start(bf16[128,1024]{1,0:T(8,128)(2,1)S(1)} %fusion.7), channel_id=1, source_target_pairs={{0,1},{1,0},{2,3},{3,2},{4,5},{5,4},{6,7},{7,6},{8,9},{9,8},{10,11... | collective-permute-start | bytes 786440 | tf_op jit(solution)/shard_map/ppermute | solution.py:315
  (13 other events, 35.8 us)
